TPU v7x, 32 devices: a whole 2x2x4 slice. The times are simulated.
32 devices in a mesh: sp: 8 (over z, core), tp: 4 (over y, x).
Axes of the slice: x: 2, y: 2, z: 4, core: 2. Of those that a mesh axis runs over, the one named last changes fastest.
Arguments:
- residual: bfloat16 [2048, 4096], P('sp', 'tp'), may hold values from -6 to 6
- pool_in: bfloat16 [2048, 2048], P('sp', 'tp'), may hold values from -6 to 6
- docs: int32 [2048], P('sp'), may hold values from 0 to 3, never falling along the last dimension, each value on 1 to 1024 neighbouring positions
- pool_weight: bfloat16 [16, 128, 128], P('tp'), may hold values from -0.5 to 0.5
- pool_gain: float32 [2048], P('tp'), may hold values from 0.1 to 1.9
- out_weight: bfloat16 [2048, 4096], P(None, 'tp'), may hold values from -0.125 to 0.125
- norm_gain: float32 [4096], replicated, may hold values from 0.1 to 1.9
- routes: int32 [2048, 2], P('sp'), may hold values from 0 to 7, all different within a row; in each aligned block of 256 rows (0 to 255, 256 to 511, ...) at most 96 rows name the same one
- route_weights: float32 [2048, 2], P('sp'), may hold values from 0.25 to 1
- w_gate: bfloat16 [8, 4096, 2048], P('sp', None, 'tp'), may hold values from -0.09375 to 0.09375
- w_up: bfloat16 [8, 4096, 2048], P('sp', None, 'tp'), may hold values from -0.09375 to 0.09375
- w_down: bfloat16 [8, 2048, 4096], P('sp', None, 'tp'), may hold values from -0.125 to 0.125
Outputs:
- layer_out: bfloat16 [2048, 4096], P('sp', 'tp')
Inputs may be any that keep to these rules, and one draw needn't show every extreme that they name: `docs`: document numbers never fall along the sequence; each document has at most 1024 positions. `routes`: each token names 2 different experts; among the tokens of one index of sp (aligned blocks of 256 rows) no expert is named more than 96 times, a bound that some block reaches.
All inputs are finite; a program needn't handle non-finite values.
Results may differ from a plain program's by a relative error of at most 0.012.
Values may be sent and summed in bfloat16 or wider, within the bound.
A program may use at most 64 MiB of HBM per device.

v0:
```python
import functools

import jax
import jax.numpy as jnp
from jax import lax
from jax.experimental import pallas as pl
from jax.experimental.pallas import tpu as pltpu
from jax.sharding import PartitionSpec as P

GD = 128
TOPK = 2
EXP_DEV = 1


EPS = 1e-06


def shifted_2(shard, axis, by):
    size = lax.axis_size(axis)
    pairs = [(i, i + by) for i in range(size) if 0 <= i + by < size]
    return lax.ppermute(shard, axis, pairs)


MESH = pl.DeviceIdType.MESH
CORES = 2


def remote(src, dst, send_sem, recv_sem, device):
    return pltpu.make_async_remote_copy(
        src_ref=src,
        dst_ref=dst,
        send_sem=send_sem,
        recv_sem=recv_sem,
        device_id=device,
        device_id_type=MESH,
    )


def greet(devices):
    barrier = pltpu.get_barrier_semaphore()
    for device in devices:
        pl.semaphore_signal(barrier, inc=1, device_id=device, device_id_type=MESH)
    pl.semaphore_wait(barrier, len(devices))


def project_kernel(
    n_tp,
    pooled,
    residual,
    gain,
    weight_hbm,
    updated,
    normed,
    gathered,
    weight,
    mine,
    sums,
    weight_sem,
    send_sem,
    recv_sem,
    sums_send,
    sums_recv,
):
    sp, tp = lax.axis_index("sp"), lax.axis_index("tp")
    width = pooled.shape[1]
    cols = residual.shape[1]
    load = pltpu.make_async_copy(weight_hbm, weight, weight_sem)
    load.start()
    peers = [lax.rem(tp + j, n_tp) for j in range(1, n_tp)]
    greet([(sp, peer) for peer in peers])
    sends = []
    for j, peer in enumerate(peers):
        sends.append(
            remote(pooled, gathered.at[tp], send_sem.at[j], recv_sem.at[tp], (sp, peer))
        )
        sends[-1].start()
    load.wait()

    def part(block, owner):
        rows = weight[pl.ds(pl.multiple_of(owner * width, width), width), :]
        return jnp.dot(block, rows, preferred_element_type=jnp.float32)

    total = part(pooled[...], tp)
    for j in range(1, n_tp):
        owner = lax.rem(tp + n_tp - j, n_tp)
        remote(
            pooled, gathered.at[owner], send_sem.at[0], recv_sem.at[owner], (sp, owner)
        ).wait_recv()
        total = total + part(gathered[owner], owner)
    new = (residual[...].astype(jnp.float32) + total).astype(jnp.bfloat16)
    updated[...] = new
    upf = new.astype(jnp.float32)
    squares = jnp.sum(upf * upf, axis=1, keepdims=True)
    own = jnp.broadcast_to(squares, (squares.shape[0], 128)).T[0:8]
    mine[...] = own
    small = []
    for j, peer in enumerate(peers):
        small.append(
            remote(mine, sums.at[tp], sums_send.at[j], sums_recv.at[tp], (sp, peer))
        )
        small[-1].start()
    for j in range(1, n_tp):
        owner = lax.rem(tp + n_tp - j, n_tp)
        remote(
            mine, sums.at[owner], sums_send.at[0], sums_recv.at[owner], (sp, owner)
        ).wait_recv()
        own = own + sums[owner]
    scale = lax.rsqrt(own / (cols * n_tp) + EPS)
    column = jnp.broadcast_to(scale[0:1], (128, scale.shape[1])).T[:, 0:1]
    normed[...] = (upf * column * gain[...]).astype(jnp.bfloat16)
    for copy in sends + small:
        copy.wait_send()


def experts_kernel(
    n_sp,
    n_tp,
    send,
    gate_hbm,
    up_hbm,
    down_hbm,
    out,
    rows,
    act,
    prod,
    w_gate,
    w_up,
    w_down,
    load_sem,
    d_send,
    d_recv,
    f_send,
    f_recv,
    a_send,
    a_recv,
    r_send,
    r_recv,
):
    sp, tp = lax.axis_index("sp"), lax.axis_index("tp")
    chips = n_sp // CORES
    my_chip, my_core = sp // CORES, sp % CORES
    cap, cols = send.shape[2], send.shape[3]
    hidden = act.shape[4]
    relay = n_tp == 4
    flat = CORES * cap

    loads = [
        pltpu.make_async_copy(gate_hbm, w_gate, load_sem.at[0]),
        pltpu.make_async_copy(up_hbm, w_up, load_sem.at[1]),
        pltpu.make_async_copy(down_hbm, w_down, load_sem.at[2]),
    ]
    for copy in loads:
        copy.start()
    greet(
        [(lax.rem(sp + j, n_sp), tp) for j in range(1, n_sp)]
        + [(sp, lax.rem(tp + j, n_tp)) for j in range(1, n_tp)]
    )

    def turn(k):
        k = (chips - k) % chips
        odd = k % 2
        return (odd * ((k + 1) // 2) + (1 - odd) * (chips - k // 2)) % chips

    def dispatch(chip, core):
        return remote(
            send.at[chip, core],
            rows.at[my_chip, tp, my_core],
            d_send.at[chip * CORES + core],
            d_recv.at[sp],
            (chip * CORES + core, tp),
        )

    own = pltpu.make_async_copy(
        send.at[my_chip, my_core], rows.at[my_chip, tp, my_core], d_recv.at[sp]
    )
    own.start()
    dispatch(my_chip, 1 - my_core).start()

    @pl.loop(1, chips)
    def _(k):
        chip = (my_chip + turn(k)) % chips
        for core in range(CORES):
            dispatch(chip, core).start()

    def spread(buf, chip, ssem, rsem):
        if relay:
            near = (2 * (tp // 2) + 1 - tp % 2, (tp + 2) % 4)
        else:
            near = [(tp + j) % n_tp for j in range(1, n_tp)]
        return [
            remote(buf.at[chip, tp], buf.at[chip, tp], ssem.at[chip, j], rsem.at[chip, tp], (sp, peer))
            for j, peer in enumerate(near)
        ]

    across = 2 * (tp // 2) + 1 - tp % 2
    along = (tp + 2) % 4

    def relays(buf, chip, ssem, rsem):
        return [
            remote(
                buf.at[chip, across, 0],
                buf.at[chip, across, 0],
                ssem.at[chip, 2],
                rsem.at[chip, n_tp],
                (sp, along),
            ),
            remote(
                buf.at[chip, along, 1],
                buf.at[chip, along, 1],
                ssem.at[chip, 3],
                rsem.at[chip, n_tp + 1],
                (sp, across),
            ),
        ]

    def arrive(buf, chip, peer, ssem, rsem):
        remote(
            buf.at[chip, peer], buf.at[chip, peer], ssem.at[chip, 0], rsem.at[chip, peer], (sp, peer)
        ).wait_recv()

    def pass_on(buf, chip, ssem, rsem):
        if relay:
            first, second = relays(buf, chip, ssem, rsem)
            arrive(buf, chip, across, ssem, rsem)
            first.start()
            arrive(buf, chip, along, ssem, rsem)
            second.start()

    def complete(buf, chip, ssem, rsem):
        if relay:
            far = 3 - tp
            for half, peer in ((0, along), (1, across)):
                remote(
                    buf.at[chip, far, half],
                    buf.at[chip, far, half],
                    ssem.at[chip, 0],
                    rsem.at[chip, n_tp + half],
                    (sp, peer),
                ).wait_recv()
        else:
            for j in range(1, n_tp):
                arrive(buf, chip, (tp + j) % n_tp, ssem, rsem)

    def source(k):
        return (my_chip + chips - turn(k)) % chips

    def worked(m):
        return source((m + 1) % chips)

    def give_back(chip, core):
        return remote(
            prod.at[chip, core],
            out.at[my_chip, my_core],
            r_send.at[chip * CORES + core],
            r_recv.at[sp],
            (chip * CORES + core, tp),
        )

    tile = min(hidden, 256)
    wide = min(cols, 256)

    @pl.loop(0, chips + 5)
    def _(i):
        @pl.when(i < chips)
        def _():
            chip = source(i)
            for core in range(CORES):
                remote(
                    send.at[chip, core],
                    rows.at[chip, tp, core],
                    d_send.at[0],
                    d_recv.at[chip * CORES + core],
                    (sp, tp),
                ).wait_recv()
            for copy in spread(rows, chip, f_send, f_recv):
                copy.start()

        @pl.when((i >= 1) & (i < chips + 1))
        def _():
            pass_on(rows, source(i - 1), f_send, f_recv)

        @pl.when(i == 2)
        def _():
            for copy in loads:
                copy.wait()

        @pl.when((i >= 3) & (i < chips + 3))
        def _():
            chip = worked(i - 3)
            complete(rows, chip, f_send, f_recv)

            @pl.loop(0, hidden // tile)
            def _(n):
                at = pl.ds(pl.multiple_of(n * tile, tile), tile)
                gate = jnp.zeros((flat, tile), jnp.float32)
                up = jnp.zeros((flat, tile), jnp.float32)
                for t in range(n_tp):
                    block = rows[chip, t].reshape(flat, cols)
                    deep = pl.ds(t * cols, cols)
                    gate += jnp.dot(block, w_gate[deep, at], preferred_element_type=jnp.float32)
                    up += jnp.dot(block, w_up[deep, at], preferred_element_type=jnp.float32)
                value = (jax.nn.silu(gate) * up).astype(jnp.bfloat16)
                act[chip, tp, :, :, at] = value.reshape(CORES, cap, tile)

            for copy in spread(act, chip, a_send, a_recv):
                copy.start()

        @pl.when((i >= 4) & (i < chips + 4))
        def _():
            pass_on(act, worked(i - 4), a_send, a_recv)

        @pl.when(i >= 5)
        def _():
            chip = worked(i - 5)
            complete(act, chip, a_send, a_recv)

            @pl.loop(0, cols // wide)
            def _(n):
                at = pl.ds(pl.multiple_of(n * wide, wide), wide)
                total = jnp.zeros((flat, wide), jnp.float32)
                for t in range(n_tp):
                    block = act[chip, t].reshape(flat, hidden)
                    total += jnp.dot(
                        block, w_down[pl.ds(t * hidden, hidden), at], preferred_element_type=jnp.float32
                    )
                prod[chip, :, :, at] = total.astype(jnp.bfloat16).reshape(CORES, cap, wide)

            @pl.when(i == chips + 4)
            def _():
                pltpu.make_async_copy(
                    prod.at[my_chip, my_core], out.at[my_chip, my_core], r_recv.at[sp]
                ).start()
                give_back(my_chip, 1 - my_core).start()

            @pl.when(i < chips + 4)
            def _():
                for core in range(CORES):
                    give_back(chip, core).start()

    dispatch(my_chip, 1 - my_core).wait_send()
    give_back(my_chip, 1 - my_core).wait_send()

    @pl.loop(1, chips)
    def _(k):
        chip = (my_chip + turn(k)) % chips
        for core in range(CORES):
            dispatch(chip, core).wait_send()
            give_back(chip, core).wait_send()

    @pl.loop(0, chips)
    def _(chip):
        for buf, ssem, rsem in ((rows, f_send, f_recv), (act, a_send, a_recv)):
            for copy in spread(buf, chip, ssem, rsem):
                copy.wait_send()
            if relay:
                for copy in relays(buf, chip, ssem, rsem):
                    copy.wait_send()
        for core in range(CORES):
            remote(
                prod.at[chip, core],
                out.at[chip, core],
                r_send.at[0],
                r_recv.at[chip * CORES + core],
                (sp, tp),
            ).wait_recv()


VMEM_LIMIT = 60 * 1024 * 1024


def project(pooled, residual, gain, weight):
    n_tp = lax.axis_size("tp")
    length, cols = residual.shape
    dma = pltpu.SemaphoreType.DMA
    vmem = pl.BlockSpec(memory_space=pltpu.VMEM)
    return pl.pallas_call(
        functools.partial(project_kernel, n_tp),
        out_shape=[jax.ShapeDtypeStruct((length, cols), jnp.bfloat16)] * 2,
        in_specs=[vmem, vmem, vmem, pl.BlockSpec(memory_space=pl.ANY)],
        out_specs=[vmem, vmem],
        scratch_shapes=[
            pltpu.VMEM((n_tp, *pooled.shape), jnp.bfloat16),
            pltpu.VMEM(weight.shape, jnp.bfloat16),
            pltpu.VMEM((8, length), jnp.float32),
            pltpu.VMEM((n_tp, 8, length), jnp.float32),
            dma,
            dma((n_tp,)),
            dma((n_tp,)),
            dma((n_tp,)),
            dma((n_tp,)),
        ],
        compiler_params=pltpu.CompilerParams(
            collective_id=0, has_side_effects=True, vmem_limit_bytes=VMEM_LIMIT
        ),
    )(pooled, residual, gain, weight)


def run_experts(send, w_gate, w_up, w_down):
    n_sp, n_tp = lax.axis_size("sp"), lax.axis_size("tp")
    chips, _, cap, cols = send.shape
    hidden = w_gate.shape[1]
    dma = pltpu.SemaphoreType.DMA
    vmem = pl.BlockSpec(memory_space=pltpu.VMEM)
    hbm = pl.BlockSpec(memory_space=pl.ANY)
    return pl.pallas_call(
        functools.partial(experts_kernel, n_sp, n_tp),
        out_shape=jax.ShapeDtypeStruct(send.shape, jnp.bfloat16),
        in_specs=[vmem, hbm, hbm, hbm],
        out_specs=vmem,
        scratch_shapes=[
            pltpu.VMEM((chips, n_tp, CORES, cap, cols), jnp.bfloat16),
            pltpu.VMEM((chips, n_tp, CORES, cap, hidden), jnp.bfloat16),
            pltpu.VMEM(send.shape, jnp.bfloat16),
            pltpu.VMEM(w_gate.shape, jnp.bfloat16),
            pltpu.VMEM(w_up.shape, jnp.bfloat16),
            pltpu.VMEM(w_down.shape, jnp.bfloat16),
            dma((3,)),
            dma((n_sp,)),
            dma((n_sp,)),
            dma((chips, n_tp)),
            dma((chips, n_tp + 2)),
            dma((chips, n_tp)),
            dma((chips, n_tp + 2)),
            dma((n_sp,)),
            dma((n_sp,)),
        ],
        compiler_params=pltpu.CompilerParams(
            collective_id=1, has_side_effects=True, vmem_limit_bytes=VMEM_LIMIT
        ),
    )(send, w_gate, w_up, w_down)


def shards(
    residual,
    pool_in,
    docs,
    pool_weight,
    pool_gain,
    out_weight,
    norm_gain,
    routes,
    route_weights,
    w_gate,
    w_up,
    w_down,
):
    length = pool_in.shape[0]
    width_loc = pool_in.shape[1]
    sp_index = lax.axis_index("sp")
    tp_index = lax.axis_index("tp")
    n_sp = lax.axis_size("sp")
    n_tp = lax.axis_size("tp")
    reach = 15
    prev_rows, prev_docs = shifted_2(
        (pool_in[length - reach :], docs[length - reach :].astype(jnp.bfloat16)), "sp", 1
    )
    extended = jnp.concatenate([prev_rows, pool_in], axis=0).astype(jnp.float32)
    ext_docs = jnp.concatenate([prev_docs.astype(jnp.float32), docs.astype(jnp.float32)])
    own_docs = docs.astype(jnp.float32)
    places = sp_index * length + jnp.arange(length)
    groups_loc = width_loc // GD
    group_of = tp_index * groups_loc + jnp.arange(width_loc) // GD
    span = 2 ** (1 + group_of % 4)
    totals = jnp.zeros((length, width_loc), jnp.float32)
    counts = jnp.zeros((length, width_loc), jnp.float32)
    for offset in range(16):
        shifted = extended[reach - offset : reach - offset + length]
        prior = ext_docs[reach - offset : reach - offset + length]
        same = ((places >= offset) & (prior == own_docs)).astype(jnp.float32)[:, None]
        weight = same * (offset < span).astype(jnp.float32)[None, :]
        totals = totals + weight * shifted
        counts = counts + weight
    diff = (totals / counts - extended[reach:]).astype(jnp.bfloat16)
    mixed = jnp.einsum(
        "tgc,gcd->tgd",
        diff.reshape(length, groups_loc, GD),
        pool_weight,
        preferred_element_type=jnp.float32,
    )
    pooled = (mixed.reshape(length, width_loc) * pool_gain).astype(jnp.bfloat16)
    cols = residual.shape[1]
    experts = n_sp * EXP_DEV
    slots_cap = length * TOPK * 3 // (2 * experts)
    ids = routes.reshape(-1)
    onehot = (ids[:, None] == jnp.arange(experts)[None, :]).astype(jnp.int32)
    rank = jnp.sum(onehot * (jnp.cumsum(onehot, axis=0) - 1), axis=1)
    slot = (ids * slots_cap + rank).reshape(length, TOPK)
    gain_cols = lax.dynamic_slice_in_dim(norm_gain, tp_index * cols, cols, 0)
    updated, normed = project(pooled, residual, gain_cols[None, :], out_weight)
    places_all = jnp.arange(experts * slots_cap)
    picks = [(slot[:, k : k + 1] == places_all[None, :]).astype(jnp.bfloat16) for k in range(TOPK)]
    send = lax.dot_general(
        sum(picks), normed, (((0,), (0,)), ((), ())), preferred_element_type=jnp.float32
    ).astype(jnp.bfloat16)
    returned = run_experts(
        send.reshape(n_sp // CORES, CORES, slots_cap, cols), w_gate[0], w_up[0], w_down[0]
    ).reshape(-1, cols)
    total = jnp.zeros((length, cols), jnp.float32)
    for k in range(TOPK):
        row = jnp.dot(picks[k], returned, preferred_element_type=jnp.float32)
        total = total + route_weights[:, k : k + 1] * row
    combined = updated.astype(jnp.float32) + total
    return combined.astype(jnp.bfloat16)


def solution(mesh):
    placed = (
        P("sp", "tp"),
        P("sp", "tp"),
        P("sp"),
        P("tp", None, None),
        P("tp"),
        P(None, "tp"),
        P(),
        P("sp", None),
        P("sp", None),
        P("sp", None, "tp"),
        P("sp", None, "tp"),
        P("sp", None, "tp"),
    )
    return jax.shard_map(
        shards, mesh=mesh, in_specs=placed, out_specs=P("sp", "tp"), check_vma=False
    )
```

profile of v0, /device:TPU:1, one launch (start us, length us, event | category | flops | bytes accessed | tf_op | source)
XLA Modules:
  0.0 158.3 jit_solution(9043108121100167984)
XLA Ops:
  0.0 0.0 copy-start
  0.0 0.8 fusion.45
  0.8 0.1 slice.121
  0.8 4.6 %collective-permute-start.1 = (bf16[15]{0:T(256)(128)(2,1)S(1)}, bf16[15]{0:T(256)(128)(2,1)S(1)}, u32[]{:S(2)}, u32[]{:S(2)}) collective-permute-start(bf16[15]{0:T(256)(128)(2,1)S(1)} %slice.121), channel_id=1, source_target_pairs={{0,4},{4,8},{8,12},{12,16},{16,20},{20,24},{24,28},{1,5},{5,9},{9,... | collective-permute-start | bytes 98 | tf_op jit(solution)/shard_map/ppermute | solution.py:21
  5.4 0.7 slice.119
  6.1 1.9 %collective-permute-start = (bf16[15,512]{1,0:T(8,128)(2,1)S(1)}, bf16[15,512]{1,0:T(8,128)(2,1)S(1)}, u32[]{:S(2)}, u32[]{:S(2)}) collective-permute-start(bf16[15,512]{1,0:T(8,128)(2,1)S(1)} %slice.119), channel_id=1, source_target_pairs={{0,4},{4,8},{8,12},{12,16},{16,20},{20,24},{24,28},{1,5},{5,9},{9,... | collective-permute-start | bytes 46088 | tf_op jit(solution)/shard_map/ppermute | solution.py:21
  8.3 0.8 copy.33
  9.1 0.1 eq.125
  9.2 0.1 eq.121
  9.4 1.1 reduce-window.6
  10.5 0.2 slice_reduce_fusion
  10.8 0.1 fusion.34
  10.9 0.1 reduce_sum.12
  11.0 0.1 copy.35
  11.1 0.7 multiply_add_fusion.15
  11.8 0.8 fusion.43
  12.6 1.3 dynamic_slice.3
  13.9 0.0 collective-permute-done.1
  13.9 0.1 pad_maximum_fusion
  13.9 0.8 and_convert_fusion.14
  14.7 0.0 collective-permute-done
  14.7 1.0 maximum_convert_fusion
  15.8 0.0 copy-done
  15.8 0.0 copy-start.3
  15.8 2.2 %fusion.30 = f32[4,256,128]{1,2,0:T(8,128)S(1)} fusion(bf16[4,128,128]{2,1,0:T(8,128)(2,1)S(1)} %copy-done, f32[271,512]{1,0:T(8,128)S(1)} %maximum_convert_fusion, f32[512]{0:T(512)S(1)} %get-tuple-element.31, f32[256]{0:T(256)S(1)} %get-tuple-element.10, f32[512]{0:T(512)S(1)} %get-tuple-element.32, f32[256]{0:T(256)S(1)} %get-tuple-element.11, ...), kind=kOutput, calls=%fused_computation.66 | convolution fusion | flops 42074112 | bytes 9093120 | tf_op jit(solution)/shard_map/tgc,gcd->tgd/dot_general | solution.py:474
  18.0 0.2 copy.37
  18.2 0.0 copy-done.3
  18.2 0.7 multiply_convert_fusion.pooled
  18.9 20.5 %shard_map.118 = (bf16[256,1024]{1,0:T(8,128)(2,1)}, bf16[256,1024]{1,0:T(8,128)(2,1)}) custom-call(bf16[256,512]{1,0:T(8,128)(2,1)} %multiply_convert_fusion.pooled, bf16[256,1024]{1,0:T(8,128)(2,1)} %residual.1, f32[1,1024]{1,0:T(1,128)} %bitcast.37, bf16[2048,1024]{1,0:T(8,128)(2,1)} %weight_hbm.1), custom_call_target="tpu_custom_call" | custom-call | tf_op jit(solution)/shard_map/pallas_call | solution.py:376
  39.4 2.9 %convolution_convert_fusion = bf16[768,1024]{1,0:T(8,128)(2,1)} fusion(bf16[256,1024]{1,0:T(8,128)(2,1)} %get-tuple-element.8, s32[256]{0:T(256)S(1)} %bitcast.38, s32[256]{0:T(256)S(1)} %bitcast.41), kind=kOutput, calls=%fused_computation | convolution fusion | flops 405012480 | bytes 2099200 | tf_op jit(solution)/shard_map/dot_general | solution.py:492
  42.4 112.2 %shard_map.119 = bf16[4,2,96,1024]{3,2,1,0:T(8,128)(2,1)} custom-call(bf16[4,2,96,1024]{3,2,1,0:T(8,128)(2,1)} %bitcast.35, bf16[4096,512]{1,0:T(8,128)(2,1)} %bitcast.32, bf16[4096,512]{1,0:T(8,128)(2,1)} %bitcast.33, bf16[2048,1024]{1,0:T(8,128)(2,1)} %bitcast.34), custom_call_target="tpu_custom_call" | custom-call | tf_op jit(solution)/shard_map/pallas_call | solution.py:405
  154.6 0.0 copy-start.1
  154.6 0.0 copy-start.2
  154.6 2.2 %convolution_multiply_fusion.1 = f32[256,1024]{1,0:T(8,128)S(1)} fusion(bf16[768,1024]{1,0:T(8,128)(2,1)} %bitcast.30, f32[256]{0:T(256)S(1)} %bitcast.43, s32[256]{0:T(256)S(1)} %bitcast.42), kind=kOutput, calls=%fused_computation.4 | convolution fusion | flops 403111936 | bytes 2623488 | tf_op jit(solution)/shard_map/dot_general | solution.py:500
  156.8 0.0 copy-done.1
  156.8 0.0 copy-done.2
  156.8 1.5 fusion.2
  (13 shorter events, 0.2 us)
Async XLA Ops:
  0.0 15.8 %copy-start = (bf16[4,128,128]{2,1,0:T(8,128)(2,1)S(1)}, bf16[4,128,128]{2,1,0:T(8,128)(2,1)}, u32[]{:S(2)}) copy-start(bf16[4,128,128]{2,1,0:T(8,128)(2,1)} %param.15) | copy-start | bytes 393220
  0.8 13.0 %collective-permute-start.1 = (bf16[15]{0:T(256)(128)(2,1)S(1)}, bf16[15]{0:T(256)(128)(2,1)S(1)}, u32[]{:S(2)}, u32[]{:S(2)}) collective-permute-start(bf16[15]{0:T(256)(128)(2,1)S(1)} %slice.121), channel_id=1, source_target_pairs={{0,4},{4,8},{8,12},{12,16},{16,20},{20,24},{24,28},{1,5},{5,9},{9,... | collective-permute-start | bytes 98 | tf_op jit(solution)/shard_map/ppermute | solution.py:21
  6.1 8.6 %collective-permute-start = (bf16[15,512]{1,0:T(8,128)(2,1)S(1)}, bf16[15,512]{1,0:T(8,128)(2,1)S(1)}, u32[]{:S(2)}, u32[]{:S(2)}) collective-permute-start(bf16[15,512]{1,0:T(8,128)(2,1)S(1)} %slice.119), channel_id=1, source_target_pairs={{0,4},{4,8},{8,12},{12,16},{16,20},{20,24},{24,28},{1,5},{5,9},{9,... | collective-permute-start | bytes 46088 | tf_op jit(solution)/shard_map/ppermute | solution.py:21
  15.8 2.4 %copy-start.3 = (f32[512]{0:T(512)S(1)}, f32[512]{0:T(512)}, u32[]{:S(2)}) copy-start(f32[512]{0:T(512)} %param.16) | copy-start | bytes 6148
  154.6 2.2 %copy-start.1 = (bf16[4,2,96,1024]{3,2,1,0:T(8,128)(2,1)S(1)}, bf16[4,2,96,1024]{3,2,1,0:T(8,128)(2,1)}, u32[]{:S(2)}) copy-start(bf16[4,2,96,1024]{3,2,1,0:T(8,128)(2,1)} %shard_map.119) | copy-start | bytes 4718596
  154.6 2.2 %copy-start.2 = (bf16[256,1024]{1,0:T(8,128)(2,1)S(1)}, bf16[256,1024]{1,0:T(8,128)(2,1)}, u32[]{:S(2)}) copy-start(bf16[256,1024]{1,0:T(8,128)(2,1)} %get-tuple-element.7) | copy-start | bytes 1572868
where the time goes:
time: 159 us; the launch traced here: 158 us
  Pallas kernels  133 us (84%)
  matrix products  8.79 us (6%)
  starting transfers between devices  6.48 us (4%)
  other arithmetic  5.53 us (3%)
  local copies, waits for them, and re-layouts  4.6 us (3%)
    pallas_call x1, Pallas kernels, run_experts(): pl.pallas_call(functools.partial(experts_kernel, n_sp, n_tp), out_shape=j...  112 us
    pallas_call x1, Pallas kernels, project(): pl.pallas_call(functools.partial(project_kernel, n_tp), out_shape=[jax.Sh...  20.5 us
    ppermute x2, starting transfers between devices, shifted_2(): return lax.ppermute(shard, axis, pairs)  6.48 us
    dot_general x2, matrix products, shards(): row = jnp.dot(picks[k], returned, preferred_element_type=jnp.float32)  3.63 us
  transfers between devices with their start and end apart: 2, of which 0 were waited for; matrix products, arithmetic and copies ran while one was open for 5% of the time, Pallas kernels for 0%

commit v1 on v0

v1 whole, which is shorter than its diff:
```python
import functools

import jax
import jax.numpy as jnp
from jax import lax
from jax.experimental import pallas as pl
from jax.experimental.pallas import tpu as pltpu
from jax.sharding import PartitionSpec as P

GD = 128
TOPK = 2
EPS = 1e-06
MESH = pl.DeviceIdType.MESH
CORES = 2
LANES = 128
TAIL = 16
VMEM_LIMIT = 62 * 1024 * 1024


def remote(src, dst, send_sem, recv_sem, device):
    return pltpu.make_async_remote_copy(
        src_ref=src,
        dst_ref=dst,
        send_sem=send_sem,
        recv_sem=recv_sem,
        device_id=device,
        device_id_type=MESH,
    )


class Spread:
    def __init__(self, n_tp, sp, tp, block, send_sem, recv_sem):
        self.n_tp, self.sp, self.tp = n_tp, sp, tp
        self.block, self.send_sem, self.recv_sem = block, send_sem, recv_sem
        self.relay = n_tp == 4
        self.across = 2 * (tp // 2) + 1 - tp % 2
        self.along = (tp + 2) % 4

    def copy(self, owner, piece, sem, peer):
        ref = self.block(owner, piece)
        return remote(ref, ref, self.send_sem(sem), self.recv_sem(owner, piece), (self.sp, peer))

    def direct(self):
        if self.relay:
            return [
                self.copy(self.tp, 0, 0, self.across),
                self.copy(self.tp, 1, 1, self.along),
                self.copy(self.tp, 1, 2, self.across),
                self.copy(self.tp, 0, 3, self.along),
            ]
        return [
            self.copy(self.tp, 0, j - 1, lax.rem(self.tp + j, self.n_tp)) for j in range(1, self.n_tp)
        ]

    def start(self):
        for copy in self.direct():
            copy.start()

    def relays(self):
        return [
            self.copy(self.across, 0, 4, self.along),
            self.copy(self.along, 1, 5, self.across),
        ]

    def arrive(self, owner, piece):
        self.copy(owner, piece, 0, self.across if self.relay else owner).wait_recv()

    def pass_on(self):
        if self.relay:
            first, second = self.relays()
            self.arrive(self.across, 0)
            first.start()
            self.arrive(self.along, 1)
            second.start()

    def finish_near(self):
        if self.relay:
            self.arrive(self.across, 1)
            self.arrive(self.along, 0)

    def finish(self):
        if self.relay:
            far = 3 - self.tp
            self.arrive(far, 0)
            self.arrive(far, 1)
        else:
            for j in range(1, self.n_tp):
                self.arrive(lax.rem(self.tp + j, self.n_tp), 0)

    def sent(self):
        for copy in self.direct() + (self.relays() if self.relay else []):
            copy.wait_send()


def layer_kernel(
    n_sp,
    n_tp,
    residual,
    pool_in,
    docs,
    pool_weight,
    pool_gain,
    norm_gain,
    routes,
    route_weights,
    wout_hbm,
    gate_hbm,
    up_hbm,
    down_hbm,
    out,
    ext,
    halo,
    halo_docs,
    gathered,
    acc,
    mine,
    sums,
    send,
    rows,
    act,
    prod,
    ret,
    wout,
    w_gate,
    w_up,
    w_down,
    load_sem,
    h_send,
    h_recv,
    p_send,
    p_recv,
    s_send,
    s_recv,
    d_send,
    d_recv,
    f_send,
    f_recv,
    a_send,
    a_recv,
    r_send,
    r_recv,
):
    sp, tp = lax.axis_index("sp"), lax.axis_index("tp")
    chips = n_sp // CORES
    my_chip, my_core = sp // CORES, sp % CORES
    length, width = pool_in.shape
    cols = residual.shape[1]
    cap = send.shape[2]
    hidden = act.shape[4]
    flat = CORES * cap
    experts = n_sp
    relay = n_tp == 4

    loads = [
        pltpu.make_async_copy(wout_hbm, wout, load_sem.at[0]),
        pltpu.make_async_copy(gate_hbm, w_gate, load_sem.at[1]),
        pltpu.make_async_copy(up_hbm, w_up, load_sem.at[2]),
        pltpu.make_async_copy(down_hbm, w_down, load_sem.at[3]),
    ]
    for copy in loads:
        copy.start()

    barrier = pltpu.get_barrier_semaphore()
    peers = [(lax.rem(sp + j, n_sp), tp) for j in range(1, n_sp)]
    peers += [(sp, lax.rem(tp + j, n_tp)) for j in range(1, n_tp)]
    for device in peers:
        pl.semaphore_signal(barrier, inc=1, device_id=device, device_id_type=MESH)

    high = max(16, experts)
    route = [routes[k : k + 1, :] for k in range(TOPK)]
    expert = lax.broadcasted_iota(jnp.int32, (high, length), 0)
    used = sum((expert == route[k]).astype(jnp.float32) for k in range(TOPK))
    before = lax.broadcasted_iota(jnp.int32, (length, length), 0) < lax.broadcasted_iota(
        jnp.int32, (length, length), 1
    )
    taken = jnp.dot(
        used.astype(jnp.bfloat16), before.astype(jnp.bfloat16), preferred_element_type=jnp.float32
    )
    slot = []
    for k in range(TOPK):
        rank = jnp.sum(jnp.where(expert == route[k], taken, 0.0), axis=0, keepdims=True)
        slot.append(route[k].astype(jnp.float32) * cap + rank)
    doc_row = docs[...].astype(jnp.float32)
    line = lax.broadcasted_iota(jnp.int32, (LANES, length), 0)
    table = jnp.where(line == 0, doc_row, 0.0)
    for k in range(TOPK):
        table = jnp.where(line == 1 + k, slot[k], table)
        table = jnp.where(line == 1 + TOPK + k, route_weights[k : k + 1, :], table)
    columns = table.T
    doc_column = columns[:, 0:1]
    slot_column = [columns[:, 1 + k : 2 + k] for k in range(TOPK)]
    weight_column = [columns[:, 1 + TOPK + k : 2 + TOPK + k] for k in range(TOPK)]

    ext[0 : LANES - TAIL, :] = jnp.zeros((LANES - TAIL, width), jnp.bfloat16)
    ext[LANES:, :] = pool_in[...]

    pl.semaphore_wait(barrier, len(peers))

    following = (lax.rem(sp + 1, n_sp), tp)
    halo_copies = [
        remote(docs.at[:, length - LANES :], halo_docs, h_send.at[0], h_recv.at[0], following),
        remote(pool_in.at[length - TAIL :, :], halo, h_send.at[1], h_recv.at[1], following),
    ]
    for copy in halo_copies:
        copy.start()

    blocks = length // LANES
    away = (
        LANES
        + lax.broadcasted_iota(jnp.int32, (LANES, 2 * LANES), 0)
        - lax.broadcasted_iota(jnp.int32, (LANES, 2 * LANES), 1)
    )
    half = LANES // 2

    def pooled_spread(b):
        def block(owner, piece):
            if relay:
                return gathered.at[owner, pl.ds(b * LANES + piece * half, half), :]
            return gathered.at[owner, pl.ds(b * LANES, LANES), :]

        return Spread(
            n_tp, sp, tp, block, lambda i: p_send.at[b, i], lambda owner, piece: p_recv.at[b, owner, piece]
        )

    def pool(b, prior):
        low = b * LANES
        near = (doc_column[low : low + LANES, :] == prior) & (away >= 0)
        groups = width // GD
        for g in range(groups):
            if groups % 4 == 0:
                span = 2 << (g % 4)
            else:
                span = lax.shift_left(jnp.int32(2), (tp * groups + g) % 4)
            weight = (near & (away < span)).astype(jnp.float32)
            at = slice(g * GD, (g + 1) * GD)
            count = jnp.sum(weight, axis=1, keepdims=True)
            total = jnp.dot(
                weight.astype(jnp.bfloat16), ext[low : low + 2 * LANES, at], preferred_element_type=jnp.float32
            )
            own = ext[low + LANES : low + 2 * LANES, at].astype(jnp.float32)
            diff = (total / count - own).astype(jnp.bfloat16)
            mixed = jnp.dot(diff, pool_weight[g], preferred_element_type=jnp.float32)
            gathered[tp, low : low + LANES, at] = (mixed * pool_gain[:, at]).astype(jnp.bfloat16)
        pooled_spread(b).start()

    for b in range(1, blocks):
        pool(b, doc_row[:, (b - 1) * LANES : (b + 1) * LANES])
    for copy in halo_copies:
        copy.wait_recv()
    ext[LANES - TAIL : LANES, :] = halo[...]
    first_docs = jnp.where(sp > 0, halo_docs[...].astype(jnp.float32), -1.0)
    pool(0, jnp.concatenate([first_docs, doc_row[:, :LANES]], axis=1))

    def part(owner):
        deep = pl.ds(pl.multiple_of(owner * width, width), width)
        return jnp.dot(gathered[owner], wout[deep, :], preferred_element_type=jnp.float32)

    loads[0].wait()
    acc[...] = residual[...].astype(jnp.float32) + part(tp)
    order = list(range(1, blocks)) + [0]
    for b in order:
        pooled_spread(b).pass_on()
    if relay:
        for b in order:
            pooled_spread(b).finish_near()
        acc[...] += part(2 * (tp // 2) + 1 - tp % 2)
        acc[...] += part((tp + 2) % 4)
        for b in order:
            pooled_spread(b).finish()
        acc[...] += part(3 - tp)
    else:
        for b in order:
            pooled_spread(b).finish()

        @pl.loop(1, n_tp)
        def _(j):
            acc[...] += part(lax.rem(tp + j, n_tp))

    upf = acc[...].astype(jnp.bfloat16).astype(jnp.float32)
    acc[...] = upf
    squares = jnp.sum(upf * upf, axis=1, keepdims=True)
    own = jnp.broadcast_to(squares, (length, LANES)).T[0:8]
    mine[...] = own
    small = [
        remote(mine, sums.at[tp], s_send.at[j - 1], s_recv.at[tp], (sp, lax.rem(tp + j, n_tp)))
        for j in range(1, n_tp)
    ]
    for copy in small:
        copy.start()
    for j in range(1, n_tp):
        owner = lax.rem(tp + n_tp - j, n_tp)
        remote(mine, sums.at[owner], s_send.at[0], s_recv.at[owner], (sp, owner)).wait_recv()
        own = own + sums[owner]
    scale = lax.rsqrt(own / (cols * n_tp) + EPS)
    column = jnp.broadcast_to(scale[0:1], (LANES, length)).T[:, 0:1]
    gain = norm_gain[:, pl.ds(pl.multiple_of(tp * cols, LANES), cols)]
    normed = (acc[...] * column * gain).astype(jnp.bfloat16)

    step = 1 - 2 * (my_chip // ((chips + 1) // 2))

    def source(k):
        return (my_chip + step * k + chips) % chips

    def dispatch(chip, core):
        return remote(
            send.at[chip, core],
            rows.at[my_chip, tp, my_core],
            d_send.at[chip * CORES + core],
            d_recv.at[sp],
            (chip * CORES + core, tp),
        )

    place = lax.broadcasted_iota(jnp.int32, (flat, length), 0).astype(jnp.float32)
    for k in range(chips):
        chip = source(k)
        here = place + (chip * flat).astype(jnp.float32)
        pick = sum((here == slot[j]).astype(jnp.float32) for j in range(TOPK)).astype(jnp.bfloat16)
        chosen = jnp.dot(pick, normed, preferred_element_type=jnp.float32).astype(jnp.bfloat16)
        send[chip] = chosen.reshape(CORES, cap, cols)
        if k == 0:
            rows[my_chip, tp, my_core] = send[my_chip, my_core]
            dispatch(my_chip, 1 - my_core).start()
        else:
            for core in range(CORES):
                dispatch(chip, core).start()

    def spread_of(buf, ssem, rsem, chip):
        def block(owner, piece):
            return buf.at[chip, owner, piece] if relay else buf.at[chip, owner]

        return Spread(
            n_tp, sp, tp, block, lambda i: ssem.at[chip, i], lambda owner, piece: rsem.at[chip, owner, piece]
        )

    def row_spread(chip):
        return spread_of(rows, f_send, f_recv, chip)

    def act_spread(chip):
        return spread_of(act, a_send, a_recv, chip)

    def give_back(chip, core):
        return remote(
            prod.at[chip, core],
            ret.at[my_chip, my_core],
            r_send.at[chip * CORES + core],
            r_recv.at[sp],
            (chip * CORES + core, tp),
        )

    tile = min(hidden, 256)
    wide = min(cols, 256)

    def activate(chip):
        @pl.loop(0, hidden // tile)
        def _(n):
            at = pl.ds(pl.multiple_of(n * tile, tile), tile)
            gate = jnp.zeros((flat, tile), jnp.float32)
            up = jnp.zeros((flat, tile), jnp.float32)
            for t in range(n_tp):
                block = rows[chip, t].reshape(flat, cols)
                deep = pl.ds(t * cols, cols)
                gate += jnp.dot(block, w_gate[deep, at], preferred_element_type=jnp.float32)
                up += jnp.dot(block, w_up[deep, at], preferred_element_type=jnp.float32)
            value = (jax.nn.silu(gate) * up).astype(jnp.bfloat16)
            act[chip, tp, :, :, at] = value.reshape(CORES, cap, tile)

    def produce(chip):
        @pl.loop(0, cols // wide)
        def _(n):
            at = pl.ds(pl.multiple_of(n * wide, wide), wide)
            total = jnp.zeros((flat, wide), jnp.float32)
            for t in range(n_tp):
                block = act[chip, t].reshape(flat, hidden)
                deep = pl.ds(t * hidden, hidden)
                total += jnp.dot(block, w_down[deep, at], preferred_element_type=jnp.float32)
            prod[chip, :, :, at] = total.astype(jnp.bfloat16).reshape(CORES, cap, wide)

    @pl.loop(0, chips + 2)
    def _(i):
        @pl.when(i < chips)
        def _():
            chip = source(i)
            for core in range(CORES):

                @pl.when(chip * CORES + core != sp)
                def _():
                    remote(
                        send.at[chip, core],
                        rows.at[chip, tp, core],
                        d_send.at[0],
                        d_recv.at[chip * CORES + core],
                        (chip * CORES + core, tp),
                    ).wait_recv()

            row_spread(chip).start()

        @pl.when(i == chips)
        def _():
            act_spread(my_chip).start()

        @pl.when(i == 1)
        def _():
            for copy in loads[1:]:
                copy.wait()

        @pl.when((i >= 1) & (i < chips + 1))
        def _():
            chip = source(i - 1)
            row_spread(chip).finish_near()
            row_spread(chip).finish()
            activate(chip)

            @pl.when(i >= 2)
            def _():
                act_spread(chip).start()

        @pl.when(i >= 3)
        def _():
            chip = source(i - 2)
            act_spread(chip).finish_near()
            act_spread(chip).finish()
            produce(chip)
            for core in range(CORES):
                give_back(chip, core).start()

        @pl.when(i < chips)
        def _():
            row_spread(source(i)).pass_on()

        @pl.when(i == chips)
        def _():
            act_spread(my_chip).pass_on()

        @pl.when((i >= 2) & (i < chips + 1))
        def _():
            act_spread(source(i - 1)).pass_on()

    act_spread(my_chip).finish_near()
    act_spread(my_chip).finish()
    produce(my_chip)
    give_back(my_chip, 1 - my_core).start()
    ret[my_chip, my_core] = prod[my_chip, my_core]

    lane = lax.broadcasted_iota(jnp.int32, (length, flat), 1).astype(jnp.float32)
    late = [k for k in range(1, chips) if k != chips // 2]
    for k in [chips // 2, 0] + late if chips > 1 else [0]:
        chip = source(k)
        here = lane + (chip * flat).astype(jnp.float32)
        weight = sum(
            jnp.where(slot_column[j] == here, weight_column[j], 0.0) for j in range(TOPK)
        )
        upper = weight.astype(jnp.bfloat16)
        lower = (weight - upper.astype(jnp.float32)).astype(jnp.bfloat16)
        for core in range(CORES):

            @pl.when(chip * CORES + core != sp)
            def _():
                remote(
                    prod.at[chip, core],
                    ret.at[chip, core],
                    r_send.at[0],
                    r_recv.at[chip * CORES + core],
                    (chip * CORES + core, tp),
                ).wait_recv()

        back = ret[chip].reshape(flat, cols)
        acc[...] += jnp.dot(upper, back, preferred_element_type=jnp.float32) + jnp.dot(
            lower, back, preferred_element_type=jnp.float32
        )
    out[...] = acc[...].astype(jnp.bfloat16)

    for copy in halo_copies + small:
        copy.wait_send()
    for b in range(blocks):
        pooled_spread(b).sent()
    dispatch(my_chip, 1 - my_core).wait_send()
    give_back(my_chip, 1 - my_core).wait_send()

    @pl.loop(1, chips)
    def _(k):
        for core in range(CORES):
            dispatch(source(k), core).wait_send()
            give_back(source(k), core).wait_send()

    @pl.loop(0, chips)
    def _(chip):
        row_spread(chip).sent()
        act_spread(chip).sent()


def shards(
    residual,
    pool_in,
    docs,
    pool_weight,
    pool_gain,
    out_weight,
    norm_gain,
    routes,
    route_weights,
    w_gate,
    w_up,
    w_down,
):
    length, width = pool_in.shape
    cols = residual.shape[1]
    hidden = w_gate.shape[2]
    n_sp, n_tp = lax.axis_size("sp"), lax.axis_size("tp")
    chips = n_sp // CORES
    cap = length * TOPK * 3 // (2 * n_sp)
    blocks = length // LANES
    pieces = 2 if n_tp == 4 else 1
    fan = 6 if n_tp == 4 else n_tp
    dma = pltpu.SemaphoreType.DMA
    vmem = pl.BlockSpec(memory_space=pltpu.VMEM)
    hbm = pl.BlockSpec(memory_space=pl.ANY)
    half = jnp.bfloat16
    return pl.pallas_call(
        functools.partial(layer_kernel, n_sp, n_tp),
        out_shape=jax.ShapeDtypeStruct((length, cols), half),
        in_specs=[vmem] * 8 + [hbm] * 4,
        out_specs=vmem,
        scratch_shapes=[
            pltpu.VMEM((LANES + length, width), half),
            pltpu.VMEM((TAIL, width), half),
            pltpu.VMEM((1, LANES), jnp.int32),
            pltpu.VMEM((n_tp, length, width), half),
            pltpu.VMEM((length, cols), jnp.float32),
            pltpu.VMEM((8, length), jnp.float32),
            pltpu.VMEM((n_tp, 8, length), jnp.float32),
            pltpu.VMEM((chips, CORES, cap, cols), half),
            pltpu.VMEM((chips, n_tp, CORES, cap, cols), half),
            pltpu.VMEM((chips, n_tp, CORES, cap, hidden), half),
            pltpu.VMEM((chips, CORES, cap, cols), half),
            pltpu.VMEM((chips, CORES, cap, cols), half),
            pltpu.VMEM(out_weight.shape, half),
            pltpu.VMEM(w_gate.shape[1:], half),
            pltpu.VMEM(w_up.shape[1:], half),
            pltpu.VMEM(w_down.shape[1:], half),
            dma((4,)),
            dma((2,)),
            dma((2,)),
            dma((blocks, fan)),
            dma((blocks, n_tp, pieces)),
            dma((n_tp,)),
            dma((n_tp,)),
            dma((n_sp,)),
            dma((n_sp,)),
            dma((chips, fan)),
            dma((chips, n_tp, pieces)),
            dma((chips, fan)),
            dma((chips, n_tp, pieces)),
            dma((n_sp,)),
            dma((n_sp,)),
        ],
        compiler_params=pltpu.CompilerParams(
            collective_id=0, has_side_effects=True, vmem_limit_bytes=VMEM_LIMIT
        ),
    )(
        residual,
        pool_in,
        docs.reshape(1, length),
        pool_weight,
        pool_gain.reshape(1, width),
        norm_gain.reshape(1, -1),
        routes.T,
        route_weights.T,
        out_weight,
        w_gate[0],
        w_up[0],
        w_down[0],
    )


def solution(mesh):
    placed = (
        P("sp", "tp"),
        P("sp", "tp"),
        P("sp"),
        P("tp", None, None),
        P("tp"),
        P(None, "tp"),
        P(),
        P("sp", None),
        P("sp", None),
        P("sp", None, "tp"),
        P("sp", None, "tp"),
        P("sp", None, "tp"),
    )
    return jax.shard_map(
        shards, mesh=mesh, in_specs=placed, out_specs=P("sp", "tp"), check_vma=False
    )
```

time: 159 us -> 127 us (0.80)
  matrix products: 8.79 us -> 0 us
  Pallas kernels: 133 us -> 125 us
  starting transfers between devices: 6.48 us -> 0 us
  other arithmetic: 5.53 us -> 0 us
  local copies, waits for them, and re-layouts: 4.6 us -> 1.87 us
    dot_general x4 -> x0, matrix products: 8.79 us -> none  [the longest x2 3.63 us: shards(): row = jnp.dot(picks[k], returned, preferred_element_type=jnp.float32)]
    pallas_call x2 -> x1, Pallas kernels: 133 us -> 125 us  [shards(): pl.pallas_call(functools.partial(layer_kernel, n_sp, n_tp), out_shape=jax...]
    ppermute x2 -> x0, starting transfers between devices: 6.48 us -> none  [shifted_2(): return lax.ppermute(shard, axis, pairs)]
    convert_element_type x13 -> x0, other arithmetic: 2.72 us -> none  [the longest x1 1.02 us: shards(): extended = jnp.concatenate([prev_rows, pool_in], axis=0).astype(jnp.float32)]
    another operation x3 -> x0, other arithmetic: 1.94 us -> none
    slice x5 -> x0, local copies, waits for them, and re-layouts: 1.78 us -> none  [the longest x1 0.76 us: shards(): total = total + route_weights[:, k:k + 1] * row]
  transfers between devices with their start and end apart: 2 -> 0, of which waited for: 0 -> 0; matrix products, arithmetic and copies ran while one was open for 5% -> 0% of each run, Pallas kernels for 0% -> 0%
where the time goes in v1:
time: 127 us
  Pallas kernels  125 us (98%)
  local copies, waits for them, and re-layouts  1.87 us (1%)
    pallas_call x1, Pallas kernels, shards(): pl.pallas_call(functools.partial(layer_kernel, n_sp, n_tp), out_shape=jax...  125 us

profile of v1, /device:TPU:1, one launch (start us, length us, event | category | flops | bytes accessed | tf_op | source)
XLA Modules:
  0.0 127.1 jit_solution(14812723075760665773)
XLA Ops:
  0.0 125.2 %shard_map.118 = bf16[256,1024]{1,0:T(8,128)(2,1)} custom-call(bf16[256,1024]{1,0:T(8,128)(2,1)} %residual.1, bf16[256,512]{1,0:T(8,128)(2,1)} %pool_in.1, s32[1,256]{1,0:T(1,128)} %bitcast.15, bf16[4,128,128]{2,1,0:T(8,128)(2,1)} %pool_weight.1, f32[1,512]{1,0:T(1,128)} %bitcast.12, f32[1,4096]{1,0:T(1,128)} %bitcast.11, s32[2,256]{1,0:T(2,128)} %bitcast.13, ...), custom_call_target="tpu_custom_call" | custom-call | tf_op jit(solution)/shard_map/pallas_call | solution.py:518
  125.2 1.9 %copy.14 = bf16[256,1024]{1,0:T(8,128)(2,1)} copy(bf16[256,1024]{1,0:T(8,128)(2,1)} %shard_map.118) | data formatting | bytes 1048576

commit v2 on v1

--- a/solution.py
+++ b/solution.py
@@ -90,6 +90,46 @@
     def sent(self):
         for copy in self.direct() + (self.relays() if self.relay else []):
             copy.wait_send()
+
+
+STAGES = ["D", "RD", "CD", "A", "RA", "CA"]
+MID = (
+    "D0 RD0 D3 RD3",
+    "D1 CD3 A3 RA3",
+    "D2 CA3 RD2 RD1",
+    "CD0 CD2 A2 RA2",
+    "CD1 A1 CA2 RA1",
+    "A0 CA1 RA0 CA0",
+)
+EDGE = (
+    "D0 RD0 D1 RD1",
+    "D3 CD1 RD3 D2",
+    "CD3 A3 RA3 CD0",
+    "A1 RD2 CA3 RA1",
+    "CD2 A2 CA1 RA2",
+    "CA2 A0 RA0 CA0",
+)
+
+
+def schedules(chips):
+    if chips == 4:
+        return [[(step[:-1], int(step[-1])) for step in " ".join(plan).split()] for plan in (MID, EDGE)]
+    steps = [("D", 0), ("RD", 0)]
+    for k in range(1, chips):
+        steps += [("D", k), ("RD", k), ("CD", k - 1), ("A", k - 1), ("RA", k - 1), ("CA", k - 1)]
+    last = chips - 1
+    steps += [("CD", last), ("A", last), ("RA", last), ("CA", last)]
+    return steps, steps
+
+
+def send_order(chips):
+    return [0, 1, 3, 2] if chips == 4 else list(range(chips))
+
+
+def return_orders(chips):
+    if chips == 4:
+        return [3, 2, 0, 1], [3, 1, 0, 2]
+    return [list(range(1, chips)) + [0]] * 2
 
 
 def layer_kernel(
@@ -296,10 +336,17 @@
     gain = norm_gain[:, pl.ds(pl.multiple_of(tp * cols, LANES), cols)]
     normed = (acc[...] * column * gain).astype(jnp.bfloat16)
 
-    step = 1 - 2 * (my_chip // ((chips + 1) // 2))
-
     def source(k):
-        return (my_chip + step * k + chips) % chips
+        bits = range(max(1, (chips - 1).bit_length()))
+        return sum(((my_chip // 2**b + k // 2**b) % 2) * 2**b for b in bits)
+
+    inner = ((my_chip + 1) // 2) % 2
+
+    def pick_by(i, mid, edge):
+        value = 0
+        for at, (a, b) in enumerate(zip(mid, edge)):
+            value = value + jnp.where(i == at, b + (a - b) * inner, 0)
+        return value
 
     def dispatch(chip, core):
         return remote(
@@ -311,7 +358,7 @@
         )
 
     place = lax.broadcasted_iota(jnp.int32, (flat, length), 0).astype(jnp.float32)
-    for k in range(chips):
+    for k in send_order(chips):
         chip = source(k)
         here = place + (chip * flat).astype(jnp.float32)
         pick = sum((here == slot[j]).astype(jnp.float32) for j in range(TOPK)).astype(jnp.bfloat16)
@@ -375,76 +422,70 @@
                 total += jnp.dot(block, w_down[deep, at], preferred_element_type=jnp.float32)
             prod[chip, :, :, at] = total.astype(jnp.bfloat16).reshape(CORES, cap, wide)
 
-    @pl.loop(0, chips + 2)
+    def start_rows(chip):
+        for core in range(CORES):
+
+            @pl.when(chip * CORES + core != sp)
+            def _():
+                remote(
+                    send.at[chip, core],
+                    rows.at[chip, tp, core],
+                    d_send.at[0],
+                    d_recv.at[chip * CORES + core],
+                    (chip * CORES + core, tp),
+                ).wait_recv()
+
+        row_spread(chip).start()
+
+    def finish_rows(chip):
+        row_spread(chip).finish_near()
+        row_spread(chip).finish()
+        activate(chip)
+
+    def finish_act(chip):
+        act_spread(chip).finish_near()
+        act_spread(chip).finish()
+        produce(chip)
+        for core in range(CORES):
+
+            @pl.when(chip * CORES + core != sp)
+            def _():
+                give_back(chip, core).start()
+
+        @pl.when(chip == my_chip)
+        def _():
+            ret[my_chip, my_core] = prod[my_chip, my_core]
+
+    stages = [
+        start_rows,
+        lambda chip: row_spread(chip).pass_on(),
+        finish_rows,
+        lambda chip: act_spread(chip).start(),
+        lambda chip: act_spread(chip).pass_on(),
+        finish_act,
+    ]
+    mid, edge = [
+        [STAGES.index(name) * chips + k for name, k in steps] for steps in schedules(chips)
+    ]
+    for copy in loads[1:]:
+        copy.wait()
+
+    @pl.loop(0, len(mid))
     def _(i):
-        @pl.when(i < chips)
-        def _():
-            chip = source(i)
-            for core in range(CORES):
-
-                @pl.when(chip * CORES + core != sp)
-                def _():
-                    remote(
-                        send.at[chip, core],
-                        rows.at[chip, tp, core],
-                        d_send.at[0],
-                        d_recv.at[chip * CORES + core],
-                        (chip * CORES + core, tp),
-                    ).wait_recv()
-
-            row_spread(chip).start()
-
-        @pl.when(i == chips)
-        def _():
-            act_spread(my_chip).start()
-
-        @pl.when(i == 1)
-        def _():
-            for copy in loads[1:]:
-                copy.wait()
-
-        @pl.when((i >= 1) & (i < chips + 1))
-        def _():
-            chip = source(i - 1)
-            row_spread(chip).finish_near()
-            row_spread(chip).finish()
-            activate(chip)
-
-            @pl.when(i >= 2)
+        code = pick_by(i, mid, edge)
+        chip = source(code % chips)
+        for at, stage in enumerate(stages):
+
+            @pl.when(code // chips == at)
             def _():
-                act_spread(chip).start()
-
-        @pl.when(i >= 3)
-        def _():
-            chip = source(i - 2)
-            act_spread(chip).finish_near()
-            act_spread(chip).finish()
-            produce(chip)
-            for core in range(CORES):
-                give_back(chip, core).start()
-
-        @pl.when(i < chips)
-        def _():
-            row_spread(source(i)).pass_on()
-
-        @pl.when(i == chips)
-        def _():
-            act_spread(my_chip).pass_on()
-
-        @pl.when((i >= 2) & (i < chips + 1))
-        def _():
-            act_spread(source(i - 1)).pass_on()
-
-    act_spread(my_chip).finish_near()
-    act_spread(my_chip).finish()
-    produce(my_chip)
-    give_back(my_chip, 1 - my_core).start()
-    ret[my_chip, my_core] = prod[my_chip, my_core]
+                stage(chip)
 
     lane = lax.broadcasted_iota(jnp.int32, (length, flat), 1).astype(jnp.float32)
-    late = [k for k in range(1, chips) if k != chips // 2]
-    for k in [chips // 2, 0] + late if chips > 1 else [0]:
-        chip = source(k)
+    orders = return_orders(chips)
+
+    @pl.loop(0, chips)
+    def _(i):
+        chip = source(pick_by(i, *orders))
         here = lane + (chip * flat).astype(jnp.float32)
         weight = sum(
             jnp.where(slot_column[j] == here, weight_column[j], 0.0) for j in range(TOPK)
@@ -467,7 +508,7 @@
         acc[...] += jnp.dot(upper, back, preferred_element_type=jnp.float32) + jnp.dot(
             lower, back, preferred_element_type=jnp.float32
         )
-    out[...] = acc[...].astype(jnp.bfloat16)
+    out[...] = acc[...]
 
     for copy in halo_copies + small:
         copy.wait_send()
@@ -517,7 +558,7 @@
     half = jnp.bfloat16
     return pl.pallas_call(
         functools.partial(layer_kernel, n_sp, n_tp),
-        out_shape=jax.ShapeDtypeStruct((length, cols), half),
+        out_shape=pltpu.VMEM((length, cols), jnp.float32),
         in_specs=[vmem] * 8 + [hbm] * 4,
         out_specs=vmem,
         scratch_shapes=[
@@ -569,7 +610,7 @@
         w_gate[0],
         w_up[0],
         w_down[0],
-    )
+    ).astype(half)
 
 
 def solution(mesh):

time: 127 us -> 117 us (0.921)
  Pallas kernels: 125 us -> 116 us
  local copies, waits for them, and re-layouts: 1.87 us -> 0 us
    pallas_call x1, Pallas kernels: 125 us -> 116 us  [shards(): pl.pallas_call(functools.partial(layer_kernel, n_sp, n_tp), out_shape=plt...]
    unnamed x1 -> x0, local copies, waits for them, and re-layouts: 1.87 us -> none
where the time goes in v2:
time: 117 us
  Pallas kernels  116 us (99%)
    pallas_call x1, Pallas kernels, shards(): pl.pallas_call(functools.partial(layer_kernel, n_sp, n_tp), out_shape=plt...  116 us

profile of v2, /device:TPU:1, one launch (start us, length us, event | category | flops | bytes accessed | tf_op | source)
XLA Modules:
  0.0 116.6 jit_solution(9165678593977416923)
XLA Ops:
  0.0 115.8 %shard_map.118 = f32[256,1024]{1,0:T(8,128)S(1)} custom-call(bf16[256,1024]{1,0:T(8,128)(2,1)} %residual.1, bf16[256,512]{1,0:T(8,128)(2,1)} %pool_in.1, s32[1,256]{1,0:T(1,128)} %bitcast.15, bf16[4,128,128]{2,1,0:T(8,128)(2,1)} %pool_weight.1, f32[1,512]{1,0:T(1,128)} %bitcast.12, f32[1,4096]{1,0:T(1,128)} %bitcast.11, s32[2,256]{1,0:T(2,128)} %bitcast.13, ...), custom_call_target="tpu_custom_call" | custom-call | tf_op jit(solution)/shard_map/pallas_call | solution.py:559
  115.8 0.9 convert_element_type.3

commit v3 on v1

--- a/solution.py
+++ b/solution.py
@@ -92,9 +92,59 @@
             copy.wait_send()
 
 
+STAGES = ["D", "RD", "CD", "A", "RA", "CA", "C", "Z"]
+MID = (
+    "RD0 Z0 D3 RD3",
+    "D1 CD3 A3 RA3",
+    "D2 CD0 CA3 RD2",
+    "RD1 CD2 A2 CD1",
+    "RA2 A1 CA2 RA1",
+    "A0 C3 CA1 RA0",
+    "C1 CA0 C0 C2",
+)
+EDGE = (
+    "RD0 Z0 D1 CD0",
+    "RD1 D3 RD3 D2",
+    "CD3 CD1 A3 RA3",
+    "RD2 A1 CA3 CD2",
+    "RA1 A2 CA1 RA2",
+    "A0 CA2 RA0 C3",
+    "CA0 C2 C0 C1",
+)
+
+
+def schedules(chips):
+    if chips == 4:
+        return [[(step[:-1], int(step[-1])) for step in " ".join(plan).split()] for plan in (MID, EDGE)]
+    steps = [("RD", 0)]
+    for k in range(1, chips):
+        steps += [("D", k), ("RD", k), ("CD", k - 1), ("A", k - 1), ("RA", k - 1), ("CA", k - 1)]
+    last = chips - 1
+    steps += [("CD", last), ("A", last), ("RA", last), ("CA", last)]
+    steps += [("C", k) for k in range(chips)]
+    return steps, steps
+
+
+def send_order(chips):
+    return ([0, 1], [3, 2]) if chips == 4 else (list(range(chips)), [])
+
+
 def layer_kernel(
     n_sp,
     n_tp,
+    residual_hbm,
+    pool_in_hbm,
+    docs_hbm,
+    pool_weight_hbm,
+    pool_gain_hbm,
+    norm_gain_hbm,
+    routes_hbm,
+    route_weights_hbm,
+    wout_hbm,
+    gate_hbm,
+    up_hbm,
+    down_hbm,
+    out,
     residual,
     pool_in,
     docs,
@@ -103,11 +153,6 @@
     norm_gain,
     routes,
     route_weights,
-    wout_hbm,
-    gate_hbm,
-    up_hbm,
-    down_hbm,
-    out,
     ext,
     halo,
     halo_docs,
@@ -120,10 +165,13 @@
     act,
     prod,
     ret,
+    scale_send,
+    scale_rows,
     wout,
     w_gate,
     w_up,
     w_down,
+    in_sem,
     load_sem,
     h_send,
     h_recv,
@@ -139,6 +187,9 @@
     a_recv,
     r_send,
     r_recv,
+    e_send,
+    e_recv,
+    credit,
 ):
     sp, tp = lax.axis_index("sp"), lax.axis_index("tp")
     chips = n_sp // CORES
@@ -150,6 +201,7 @@
     flat = CORES * cap
     experts = n_sp
     relay = n_tp == 4
+    room = -(-cap // LANES) * LANES
 
     loads = [
         pltpu.make_async_copy(wout_hbm, wout, load_sem.at[0]),
@@ -157,14 +209,32 @@
         pltpu.make_async_copy(up_hbm, w_up, load_sem.at[2]),
         pltpu.make_async_copy(down_hbm, w_down, load_sem.at[3]),
     ]
-    for copy in loads:
-        copy.start()
-
     barrier = pltpu.get_barrier_semaphore()
     peers = [(lax.rem(sp + j, n_sp), tp) for j in range(1, n_sp)]
     peers += [(sp, lax.rem(tp + j, n_tp)) for j in range(1, n_tp)]
     for device in peers:
         pl.semaphore_signal(barrier, inc=1, device_id=device, device_id_type=MESH)
+    inputs = [
+        pltpu.make_async_copy(src, dst, in_sem.at[at])
+        for at, (src, dst) in enumerate(
+            (
+                (routes_hbm, routes),
+                (route_weights_hbm, route_weights),
+                (docs_hbm, docs),
+                (pool_in_hbm, pool_in),
+                (pool_weight_hbm, pool_weight),
+                (pool_gain_hbm, pool_gain),
+                (norm_gain_hbm, norm_gain),
+                (residual_hbm, residual),
+            )
+        )
+    ]
+    for copy in inputs:
+        copy.start()
+    for copy in inputs:
+        copy.wait()
+    for copy in loads:
+        copy.start()
 
     high = max(16, experts)
     route = [routes[k : k + 1, :] for k in range(TOPK)]
@@ -194,16 +264,6 @@
     ext[0 : LANES - TAIL, :] = jnp.zeros((LANES - TAIL, width), jnp.bfloat16)
     ext[LANES:, :] = pool_in[...]
 
-    pl.semaphore_wait(barrier, len(peers))
-
-    following = (lax.rem(sp + 1, n_sp), tp)
-    halo_copies = [
-        remote(docs.at[:, length - LANES :], halo_docs, h_send.at[0], h_recv.at[0], following),
-        remote(pool_in.at[length - TAIL :, :], halo, h_send.at[1], h_recv.at[1], following),
-    ]
-    for copy in halo_copies:
-        copy.start()
-
     blocks = length // LANES
     away = (
         LANES
@@ -241,15 +301,39 @@
             diff = (total / count - own).astype(jnp.bfloat16)
             mixed = jnp.dot(diff, pool_weight[g], preferred_element_type=jnp.float32)
             gathered[tp, low : low + LANES, at] = (mixed * pool_gain[:, at]).astype(jnp.bfloat16)
-        pooled_spread(b).start()
 
     for b in range(1, blocks):
         pool(b, doc_row[:, (b - 1) * LANES : (b + 1) * LANES])
-    for copy in halo_copies:
-        copy.wait_recv()
+
+    pl.semaphore_wait(barrier, len(peers))
+
+    def halo_copies(to):
+        return [
+            remote(docs.at[:, length - LANES :], halo_docs, h_send.at[0], h_recv.at[0], (to, tp)),
+            remote(pool_in.at[length - TAIL :, :], halo, h_send.at[1], h_recv.at[1], (to, tp)),
+        ]
+
+    @pl.when(sp < n_sp - 1)
+    def _():
+        for copy in halo_copies(sp + 1):
+            copy.start()
+
+    for b in range(1, blocks):
+        pooled_spread(b).start()
+    @pl.when(sp == 0)
+    def _():
+        halo[...] = jnp.zeros_like(halo)
+        halo_docs[...] = jnp.full_like(halo_docs, -1)
+
+    @pl.when(sp > 0)
+    def _():
+        for copy in halo_copies(sp - 1):
+            copy.wait_recv()
+
     ext[LANES - TAIL : LANES, :] = halo[...]
-    first_docs = jnp.where(sp > 0, halo_docs[...].astype(jnp.float32), -1.0)
+    first_docs = halo_docs[...].astype(jnp.float32)
     pool(0, jnp.concatenate([first_docs, doc_row[:, :LANES]], axis=1))
+    pooled_spread(0).start()
 
     def part(owner):
         deep = pl.ds(pl.multiple_of(owner * width, width), width)
@@ -257,19 +341,19 @@
 
     loads[0].wait()
     acc[...] = residual[...].astype(jnp.float32) + part(tp)
-    order = list(range(1, blocks)) + [0]
-    for b in order:
+    late_first = list(range(1, blocks)) + [0]
+    for b in late_first:
         pooled_spread(b).pass_on()
     if relay:
-        for b in order:
+        for b in late_first:
             pooled_spread(b).finish_near()
         acc[...] += part(2 * (tp // 2) + 1 - tp % 2)
         acc[...] += part((tp + 2) % 4)
-        for b in order:
+        for b in late_first:
             pooled_spread(b).finish()
         acc[...] += part(3 - tp)
     else:
-        for b in order:
+        for b in late_first:
             pooled_spread(b).finish()
 
         @pl.loop(1, n_tp)
@@ -278,7 +362,101 @@
 
     upf = acc[...].astype(jnp.bfloat16).astype(jnp.float32)
     acc[...] = upf
-    squares = jnp.sum(upf * upf, axis=1, keepdims=True)
+    gain = norm_gain[:, pl.ds(pl.multiple_of(tp * cols, LANES), cols)]
+    plain = (acc[...] * gain).astype(jnp.bfloat16)
+
+    def source(k):
+        bits = range(max(1, (chips - 1).bit_length()))
+        return sum(((my_chip // 2**b + k // 2**b) % 2) * 2**b for b in bits)
+
+    inner = ((my_chip + 1) // 2) % 2
+
+    def pick_by(i, mid, edge):
+        value = 0
+        for at, (a, b) in enumerate(zip(mid, edge)):
+            value = value + jnp.where(i == at, b + (a - b) * inner, 0)
+        return value
+
+    def dispatch(chip, core):
+        return remote(
+            send.at[chip, core],
+            rows.at[my_chip, tp, my_core],
+            d_send.at[chip * CORES + core],
+            d_recv.at[sp],
+            (chip * CORES + core, tp),
+        )
+
+    def dispatch_scale(chip, core):
+        return remote(
+            scale_send.at[chip, core],
+            scale_rows.at[my_chip, my_core],
+            e_send.at[chip * CORES + core],
+            e_recv.at[sp],
+            (chip * CORES + core, tp),
+        )
+
+    place = lax.broadcasted_iota(jnp.int32, (flat, length), 0).astype(jnp.float32)
+
+    def choose(k):
+        chip = source(k)
+        here = place + (chip * flat).astype(jnp.float32)
+        pick = sum((here == slot[j]).astype(jnp.float32) for j in range(TOPK)).astype(jnp.bfloat16)
+        chosen = jnp.dot(pick, plain, preferred_element_type=jnp.float32).astype(jnp.bfloat16)
+        send[chip] = chosen.reshape(CORES, cap, cols)
+        if k == 0:
+            rows[my_chip, tp, my_core] = send[my_chip, my_core]
+            dispatch(my_chip, 1 - my_core).start()
+
+    def start_send(k, cores):
+        for core in cores:
+            dispatch(source(k), core).start()
+
+    def spread_of(buf, ssem, rsem, chip):
+        def block(owner, piece):
+            return buf.at[chip, owner, piece] if relay else buf.at[chip, owner]
+
+        return Spread(
+            n_tp, sp, tp, block, lambda i: ssem.at[chip, i], lambda owner, piece: rsem.at[chip, owner, piece]
+        )
+
+    def row_spread(chip):
+        return spread_of(rows, f_send, f_recv, chip)
+
+    def act_spread(chip):
+        return spread_of(act, a_send, a_recv, chip)
+
+    def start_rows(chip):
+        for core in range(CORES):
+
+            @pl.when(chip * CORES + core != sp)
+            def _():
+                remote(
+                    send.at[chip, core],
+                    rows.at[chip, tp, core],
+                    d_send.at[0],
+                    d_recv.at[chip * CORES + core],
+                    (chip * CORES + core, tp),
+                ).wait_recv()
+
+        row_spread(chip).start()
+
+    first, rest = send_order(chips)
+    held = chips == 4
+
+    def send_first(k):
+        choose(k)
+        if k:
+            start_send(k, range(CORES))
+
+    if held:
+
+        @pl.when(inner == 1)
+        def _():
+            send_first(3)
+
+    for k in first:
+        send_first(k)
+    squares = jnp.sum(acc[...] * acc[...], axis=1, keepdims=True)
     own = jnp.broadcast_to(squares, (length, LANES)).T[0:8]
     mine[...] = own
     small = [
@@ -287,61 +465,62 @@
     ]
     for copy in small:
         copy.start()
+    start_rows(my_chip)
+
     for j in range(1, n_tp):
         owner = lax.rem(tp + n_tp - j, n_tp)
         remote(mine, sums.at[owner], s_send.at[0], s_recv.at[owner], (sp, owner)).wait_recv()
         own = own + sums[owner]
-    scale = lax.rsqrt(own / (cols * n_tp) + EPS)
-    column = jnp.broadcast_to(scale[0:1], (LANES, length)).T[:, 0:1]
-    gain = norm_gain[:, pl.ds(pl.multiple_of(tp * cols, LANES), cols)]
-    normed = (acc[...] * column * gain).astype(jnp.bfloat16)
-
-    step = 1 - 2 * (my_chip // ((chips + 1) // 2))
-
-    def source(k):
-        return (my_chip + step * k + chips) % chips
-
-    def dispatch(chip, core):
+    scale = lax.rsqrt(own[0:1] / (cols * n_tp) + EPS)
+    slots_here = lax.broadcasted_iota(jnp.int32, (room, length), 0).astype(jnp.float32)
+    for k in first + rest:
+        chip = source(k)
+        for core in range(CORES):
+            here = slots_here + (chip * flat + core * cap).astype(jnp.float32)
+            mine_here = sum(jnp.where(here == slot[j], scale, 0.0) for j in range(TOPK))
+            column = jnp.sum(mine_here, axis=1, keepdims=True)
+            line = jnp.broadcast_to(column, (room, LANES)).T[0:8]
+            scale_send[chip, core] = line
+
+            @pl.when(chip * CORES + core == sp)
+            def _():
+                scale_rows[my_chip, my_core] = scale_send[my_chip, my_core]
+
+            @pl.when(chip * CORES + core != sp)
+            def _():
+                dispatch_scale(chip, core).start()
+
+    for k in rest:
+
+        @pl.when((inner == 0) | (k != 3))
+        def _():
+            choose(k)
+
+    def hold(chip):
+        @pl.when(inner == 1)
+        def _():
+            for k in (1, 3):
+                for core in range(CORES):
+                    dispatch(source(k), core).wait_send()
+                    dispatch_scale(source(k), core).wait_send()
+            for k in (1, 2, 3):
+                for core in range(CORES):
+                    pl.semaphore_signal(
+                        credit, inc=1, device_id=(source(k) * CORES + core, tp), device_id_type=MESH
+                    )
+            pl.semaphore_wait(credit, CORES)
+            start_send(2, range(CORES))
+
+        @pl.when(inner == 0)
+        def _():
+            pl.semaphore_wait(credit, 2 * CORES)
+            for k in rest:
+                start_send(k, range(CORES))
+
+    def give_back(chip, core, at=slice(None)):
         return remote(
-            send.at[chip, core],
-            rows.at[my_chip, tp, my_core],
-            d_send.at[chip * CORES + core],
-            d_recv.at[sp],
-            (chip * CORES + core, tp),
-        )
-
-    place = lax.broadcasted_iota(jnp.int32, (flat, length), 0).astype(jnp.float32)
-    for k in range(chips):
-        chip = source(k)
-        here = place + (chip * flat).astype(jnp.float32)
-        pick = sum((here == slot[j]).astype(jnp.float32) for j in range(TOPK)).astype(jnp.bfloat16)
-        chosen = jnp.dot(pick, normed, preferred_element_type=jnp.float32).astype(jnp.bfloat16)
-        send[chip] = chosen.reshape(CORES, cap, cols)
-        if k == 0:
-            rows[my_chip, tp, my_core] = send[my_chip, my_core]
-            dispatch(my_chip, 1 - my_core).start()
-        else:
-            for core in range(CORES):
-                dispatch(chip, core).start()
-
-    def spread_of(buf, ssem, rsem, chip):
-        def block(owner, piece):
-            return buf.at[chip, owner, piece] if relay else buf.at[chip, owner]
-
-        return Spread(
-            n_tp, sp, tp, block, lambda i: ssem.at[chip, i], lambda owner, piece: rsem.at[chip, owner, piece]
-        )
-
-    def row_spread(chip):
-        return spread_of(rows, f_send, f_recv, chip)
-
-    def act_spread(chip):
-        return spread_of(act, a_send, a_recv, chip)
-
-    def give_back(chip, core):
-        return remote(
-            prod.at[chip, core],
-            ret.at[my_chip, my_core],
+            prod.at[chip, core, :, at],
+            ret.at[my_chip, my_core, :, at],
             r_send.at[chip * CORES + core],
             r_recv.at[sp],
             (chip * CORES + core, tp),
@@ -351,6 +530,26 @@
     wide = min(cols, 256)
 
     def activate(chip):
+        for core in range(CORES):
+
+            @pl.when(chip * CORES + core != sp)
+            def _():
+                remote(
+                    scale_send.at[chip, core],
+                    scale_rows.at[chip, core],
+                    e_send.at[0],
+                    e_recv.at[chip * CORES + core],
+                    (chip * CORES + core, tp),
+                ).wait_recv()
+
+        column = jnp.concatenate(
+            [
+                jnp.broadcast_to(scale_rows[chip, core, 0:1], (LANES, room)).T[:cap, 0:1]
+                for core in range(CORES)
+            ],
+            axis=0,
+        )
+
         @pl.loop(0, hidden // tile)
         def _(n):
             at = pl.ds(pl.multiple_of(n * tile, tile), tile)
@@ -361,7 +560,7 @@
                 deep = pl.ds(t * cols, cols)
                 gate += jnp.dot(block, w_gate[deep, at], preferred_element_type=jnp.float32)
                 up += jnp.dot(block, w_up[deep, at], preferred_element_type=jnp.float32)
-            value = (jax.nn.silu(gate) * up).astype(jnp.bfloat16)
+            value = (jax.nn.silu(gate * column) * (up * column)).astype(jnp.bfloat16)
             act[chip, tp, :, :, at] = value.reshape(CORES, cap, tile)
 
     def produce(chip):
@@ -374,77 +573,29 @@
                 deep = pl.ds(t * hidden, hidden)
                 total += jnp.dot(block, w_down[deep, at], preferred_element_type=jnp.float32)
             prod[chip, :, :, at] = total.astype(jnp.bfloat16).reshape(CORES, cap, wide)
-
-    @pl.loop(0, chips + 2)
-    def _(i):
-        @pl.when(i < chips)
-        def _():
-            chip = source(i)
             for core in range(CORES):
 
                 @pl.when(chip * CORES + core != sp)
                 def _():
-                    remote(
-                        send.at[chip, core],
-                        rows.at[chip, tp, core],
-                        d_send.at[0],
-                        d_recv.at[chip * CORES + core],
-                        (chip * CORES + core, tp),
-                    ).wait_recv()
-
-            row_spread(chip).start()
-
-        @pl.when(i == chips)
+                    give_back(chip, core, at).start()
+
+    def finish_rows(chip):
+        row_spread(chip).finish_near()
+        row_spread(chip).finish()
+        activate(chip)
+
+    def finish_act(chip):
+        act_spread(chip).finish_near()
+        act_spread(chip).finish()
+        produce(chip)
+
+        @pl.when(chip == my_chip)
         def _():
-            act_spread(my_chip).start()
-
-        @pl.when(i == 1)
-        def _():
-            for copy in loads[1:]:
-                copy.wait()
-
-        @pl.when((i >= 1) & (i < chips + 1))
-        def _():
-            chip = source(i - 1)
-            row_spread(chip).finish_near()
-            row_spread(chip).finish()
-            activate(chip)
-
-            @pl.when(i >= 2)
-            def _():
-                act_spread(chip).start()
-
-        @pl.when(i >= 3)
-        def _():
-            chip = source(i - 2)
-            act_spread(chip).finish_near()
-            act_spread(chip).finish()
-            produce(chip)
-            for core in range(CORES):
-                give_back(chip, core).start()
-
-        @pl.when(i < chips)
-        def _():
-            row_spread(source(i)).pass_on()
-
-        @pl.when(i == chips)
-        def _():
-            act_spread(my_chip).pass_on()
-
-        @pl.when((i >= 2) & (i < chips + 1))
-        def _():
-            act_spread(source(i - 1)).pass_on()
-
-    act_spread(my_chip).finish_near()
-    act_spread(my_chip).finish()
-    produce(my_chip)
-    give_back(my_chip, 1 - my_core).start()
-    ret[my_chip, my_core] = prod[my_chip, my_core]
+            ret[my_chip, my_core] = prod[my_chip, my_core]
 
     lane = lax.broadcasted_iota(jnp.int32, (length, flat), 1).astype(jnp.float32)
-    late = [k for k in range(1, chips) if k != chips // 2]
-    for k in [chips // 2, 0] + late if chips > 1 else [0]:
-        chip = source(k)
+
+    def combine(chip):
         here = lane + (chip * flat).astype(jnp.float32)
         weight = sum(
             jnp.where(slot_column[j] == here, weight_column[j], 0.0) for j in range(TOPK)
@@ -467,20 +618,56 @@
         acc[...] += jnp.dot(upper, back, preferred_element_type=jnp.float32) + jnp.dot(
             lower, back, preferred_element_type=jnp.float32
         )
-    out[...] = acc[...].astype(jnp.bfloat16)
-
-    for copy in halo_copies + small:
+
+    stages = [
+        start_rows,
+        lambda chip: row_spread(chip).pass_on(),
+        finish_rows,
+        lambda chip: act_spread(chip).start(),
+        lambda chip: act_spread(chip).pass_on(),
+        finish_act,
+        combine,
+        hold,
+    ]
+    mid, edge = [
+        [STAGES.index(name) * chips + k for name, k in steps] for steps in schedules(chips)
+    ]
+    for copy in loads[1:]:
+        copy.wait()
+
+    @pl.loop(0, len(mid))
+    def _(i):
+        code = pick_by(i, mid, edge)
+        chip = source(code % chips)
+        for at, stage in enumerate(stages):
+
+            @pl.when(code // chips == at)
+            def _():
+                stage(chip)
+
+    out[...] = acc[...]
+
+    @pl.when(sp < n_sp - 1)
+    def _():
+        for copy in halo_copies(sp + 1):
+            copy.wait_send()
+
+    for copy in small:
         copy.wait_send()
     for b in range(blocks):
         pooled_spread(b).sent()
-    dispatch(my_chip, 1 - my_core).wait_send()
-    give_back(my_chip, 1 - my_core).wait_send()
+    for copy in (dispatch, dispatch_scale, give_back):
+        copy(my_chip, 1 - my_core).wait_send()
 
     @pl.loop(1, chips)
     def _(k):
         for core in range(CORES):
-            dispatch(source(k), core).wait_send()
             give_back(source(k), core).wait_send()
+
+            @pl.when((inner == 0) | (k == 2) | (not held))
+            def _():
+                for copy in (dispatch, dispatch_scale):
+                    copy(source(k), core).wait_send()
 
     @pl.loop(0, chips)
     def _(chip):
@@ -508,6 +695,7 @@
     n_sp, n_tp = lax.axis_size("sp"), lax.axis_size("tp")
     chips = n_sp // CORES
     cap = length * TOPK * 3 // (2 * n_sp)
+    room = -(-cap // LANES) * LANES
     blocks = length // LANES
     pieces = 2 if n_tp == 4 else 1
     fan = 6 if n_tp == 4 else n_tp
@@ -517,10 +705,18 @@
     half = jnp.bfloat16
     return pl.pallas_call(
         functools.partial(layer_kernel, n_sp, n_tp),
-        out_shape=jax.ShapeDtypeStruct((length, cols), half),
-        in_specs=[vmem] * 8 + [hbm] * 4,
+        out_shape=pltpu.VMEM((length, cols), jnp.float32),
+        in_specs=[hbm] * 12,
         out_specs=vmem,
         scratch_shapes=[
+            pltpu.VMEM((length, cols), half),
+            pltpu.VMEM((length, width), half),
+            pltpu.VMEM((1, length), jnp.int32),
+            pltpu.VMEM(pool_weight.shape, half),
+            pltpu.VMEM((1, width), jnp.float32),
+            pltpu.VMEM((1, *norm_gain.shape), jnp.float32),
+            pltpu.VMEM((TOPK, length), jnp.int32),
+            pltpu.VMEM((TOPK, length), jnp.float32),
             pltpu.VMEM((LANES + length, width), half),
             pltpu.VMEM((TAIL, width), half),
             pltpu.VMEM((1, LANES), jnp.int32),
@@ -533,10 +729,13 @@
             pltpu.VMEM((chips, n_tp, CORES, cap, hidden), half),
             pltpu.VMEM((chips, CORES, cap, cols), half),
             pltpu.VMEM((chips, CORES, cap, cols), half),
+            pltpu.VMEM((chips, CORES, 8, room), jnp.float32),
+            pltpu.VMEM((chips, CORES, 8, room), jnp.float32),
             pltpu.VMEM(out_weight.shape, half),
             pltpu.VMEM(w_gate.shape[1:], half),
             pltpu.VMEM(w_up.shape[1:], half),
             pltpu.VMEM(w_down.shape[1:], half),
+            dma((8,)),
             dma((4,)),
             dma((2,)),
             dma((2,)),
@@ -552,6 +751,9 @@
             dma((chips, n_tp, pieces)),
             dma((n_sp,)),
             dma((n_sp,)),
+            dma((n_sp,)),
+            dma((n_sp,)),
+            pltpu.SemaphoreType.REGULAR,
         ],
         compiler_params=pltpu.CompilerParams(
             collective_id=0, has_side_effects=True, vmem_limit_bytes=VMEM_LIMIT
@@ -569,7 +771,7 @@
         w_gate[0],
         w_up[0],
         w_down[0],
-    )
+    ).astype(half)
 
 
 def solution(mesh):

time: 127 us -> 106 us (0.83)
  Pallas kernels: 125 us -> 104 us
  local copies, waits for them, and re-layouts: 1.87 us -> 0 us
    pallas_call x1, Pallas kernels: 125 us -> 104 us  [shards(): pl.pallas_call(functools.partial(layer_kernel, n_sp, n_tp), out_shape=plt...]
    unnamed x1 -> x0, local copies, waits for them, and re-layouts: 1.87 us -> none
where the time goes in v3:
time: 106 us; the launch traced here: 105 us
  Pallas kernels  104 us (98%)
    pallas_call x1, Pallas kernels, shards(): pl.pallas_call(functools.partial(layer_kernel, n_sp, n_tp), out_shape=plt...  104 us

profile of v3, /device:TPU:1, one launch (start us, length us, event | category | flops | bytes accessed | tf_op | source)
XLA Modules:
  0.0 105.2 jit_solution(8701864596793650065)
XLA Ops:
  0.0 104.3 %shard_map.118 = f32[256,1024]{1,0:T(8,128)S(1)} custom-call(bf16[256,1024]{1,0:T(8,128)(2,1)} %residual_hbm.1, bf16[256,512]{1,0:T(8,128)(2,1)} %pool_in_hbm.1, s32[1,256]{1,0:T(1,128)} %bitcast.15, bf16[4,128,128]{2,1,0:T(8,128)(2,1)} %pool_weight_hbm.1, f32[1,512]{1,0:T(1,128)} %bitcast.12, f32[1,4096]{1,0:T(1,128)} %bitcast.11, s32[2,256]{1,0:T(2,128)} %bitcast.13, ...), custom_call_target="tpu_custom_call" | custom-call | tf_op jit(solution)/shard_map/pallas_call | solution.py:706
  104.3 0.9 convert_element_type.3

commit v4 on v3

--- a/solution.py
+++ b/solution.py
@@ -29,70 +29,57 @@
 
 
 class Spread:
-    def __init__(self, n_tp, sp, tp, block, send_sem, recv_sem):
+    def __init__(self, n_tp, sp, tp, block, blocks, send_sem, recv_sem):
         self.n_tp, self.sp, self.tp = n_tp, sp, tp
-        self.block, self.send_sem, self.recv_sem = block, send_sem, recv_sem
+        self.block, self.blocks, self.send_sem, self.recv_sem = block, blocks, send_sem, recv_sem
         self.relay = n_tp == 4
         self.across = 2 * (tp // 2) + 1 - tp % 2
         self.along = (tp + 2) % 4
-
-    def copy(self, owner, piece, sem, peer):
+        self.other = self.across if self.relay else lax.rem(tp + 1, n_tp)
+
+    def copy(self, owner, piece, group, peer):
         ref = self.block(owner, piece)
-        return remote(ref, ref, self.send_sem(sem), self.recv_sem(owner, piece), (self.sp, peer))
+        return remote(ref, ref, self.send_sem, self.recv_sem(group), (self.sp, peer))
 
     def direct(self):
         if self.relay:
             return [
                 self.copy(self.tp, 0, 0, self.across),
-                self.copy(self.tp, 1, 1, self.along),
-                self.copy(self.tp, 1, 2, self.across),
-                self.copy(self.tp, 0, 3, self.along),
+                self.copy(self.tp, 1, 0, self.along),
+                self.copy(self.tp, 1, 1, self.across),
+                self.copy(self.tp, 0, 1, self.along),
             ]
-        return [
-            self.copy(self.tp, 0, j - 1, lax.rem(self.tp + j, self.n_tp)) for j in range(1, self.n_tp)
-        ]
+        return [self.copy(self.tp, 0, 0, lax.rem(self.tp + j, self.n_tp)) for j in range(1, self.n_tp)]
 
     def start(self):
         for copy in self.direct():
             copy.start()
 
-    def relays(self):
-        return [
-            self.copy(self.across, 0, 4, self.along),
-            self.copy(self.along, 1, 5, self.across),
-        ]
-
-    def arrive(self, owner, piece):
-        self.copy(owner, piece, 0, self.across if self.relay else owner).wait_recv()
+    def all_of(self, group, count):
+        ref = self.blocks(count)
+        return remote(ref, ref, self.send_sem, self.recv_sem(group), (self.sp, self.other))
 
     def pass_on(self):
         if self.relay:
-            first, second = self.relays()
-            self.arrive(self.across, 0)
-            first.start()
-            self.arrive(self.along, 1)
-            second.start()
+            self.all_of(0, 1).wait_recv()
+            self.copy(self.across, 0, 2, self.along).start()
+            self.copy(self.along, 1, 2, self.across).start()
 
     def finish_near(self):
         if self.relay:
-            self.arrive(self.across, 1)
-            self.arrive(self.along, 0)
+            self.all_of(1, 1).wait_recv()
 
     def finish(self):
         if self.relay:
-            far = 3 - self.tp
-            self.arrive(far, 0)
-            self.arrive(far, 1)
+            self.all_of(2, 1).wait_recv()
         else:
-            for j in range(1, self.n_tp):
-                self.arrive(lax.rem(self.tp + j, self.n_tp), 0)
+            self.all_of(0, self.n_tp - 1).wait_recv()
 
     def sent(self):
-        for copy in self.direct() + (self.relays() if self.relay else []):
-            copy.wait_send()
-
-
-STAGES = ["D", "RD", "CD", "A", "RA", "CA", "C", "Z"]
+        self.all_of(0, self.n_tp - 1).wait_send()
+
+
+STAGES = ["D", "RD", "CD", "A", "RA", "CA", "C", "Z", "E", "W"]
 MID = (
     "RD0 Z0 D3 RD3",
     "D1 CD3 A3 RA3",
@@ -100,7 +87,8 @@
     "RD1 CD2 A2 CD1",
     "RA2 A1 CA2 RA1",
     "A0 C3 CA1 RA0",
-    "C1 CA0 C0 C2",
+    "C1 W0 CA0 C0",
+    "E2",
 )
 EDGE = (
     "RD0 Z0 D1 CD0",
@@ -109,7 +97,8 @@
     "RD2 A1 CA3 CD2",
     "RA1 A2 CA1 RA2",
     "A0 CA2 RA0 C3",
-    "CA0 C2 C0 C1",
+    "W0 CA0 C2 C0",
+    "E1",
 )
 
 
@@ -121,7 +110,7 @@
         steps += [("D", k), ("RD", k), ("CD", k - 1), ("A", k - 1), ("RA", k - 1), ("CA", k - 1)]
     last = chips - 1
     steps += [("CD", last), ("A", last), ("RA", last), ("CA", last)]
-    steps += [("C", k) for k in range(chips)]
+    steps += [("C", k) for k in range(chips - 1)] + [("W", 0), ("E", last)]
     return steps, steps
 
 
@@ -167,6 +156,7 @@
     ret,
     scale_send,
     scale_rows,
+    partial,
     wout,
     w_gate,
     w_up,
@@ -231,36 +221,11 @@
     ]
     for copy in inputs:
         copy.start()
-    for copy in inputs:
+    for copy in inputs[2:6]:
         copy.wait()
-    for copy in loads:
-        copy.start()
-
-    high = max(16, experts)
-    route = [routes[k : k + 1, :] for k in range(TOPK)]
-    expert = lax.broadcasted_iota(jnp.int32, (high, length), 0)
-    used = sum((expert == route[k]).astype(jnp.float32) for k in range(TOPK))
-    before = lax.broadcasted_iota(jnp.int32, (length, length), 0) < lax.broadcasted_iota(
-        jnp.int32, (length, length), 1
-    )
-    taken = jnp.dot(
-        used.astype(jnp.bfloat16), before.astype(jnp.bfloat16), preferred_element_type=jnp.float32
-    )
-    slot = []
-    for k in range(TOPK):
-        rank = jnp.sum(jnp.where(expert == route[k], taken, 0.0), axis=0, keepdims=True)
-        slot.append(route[k].astype(jnp.float32) * cap + rank)
+
     doc_row = docs[...].astype(jnp.float32)
-    line = lax.broadcasted_iota(jnp.int32, (LANES, length), 0)
-    table = jnp.where(line == 0, doc_row, 0.0)
-    for k in range(TOPK):
-        table = jnp.where(line == 1 + k, slot[k], table)
-        table = jnp.where(line == 1 + TOPK + k, route_weights[k : k + 1, :], table)
-    columns = table.T
-    doc_column = columns[:, 0:1]
-    slot_column = [columns[:, 1 + k : 2 + k] for k in range(TOPK)]
-    weight_column = [columns[:, 1 + TOPK + k : 2 + TOPK + k] for k in range(TOPK)]
-
+    doc_column = jnp.broadcast_to(doc_row, (LANES, length)).T[:, 0:1]
     ext[0 : LANES - TAIL, :] = jnp.zeros((LANES - TAIL, width), jnp.bfloat16)
     ext[LANES:, :] = pool_in[...]
 
@@ -278,9 +243,10 @@
                 return gathered.at[owner, pl.ds(b * LANES + piece * half, half), :]
             return gathered.at[owner, pl.ds(b * LANES, LANES), :]
 
-        return Spread(
-            n_tp, sp, tp, block, lambda i: p_send.at[b, i], lambda owner, piece: p_recv.at[b, owner, piece]
-        )
+        def several(count):
+            return gathered.at[pl.ds(0, count), pl.ds(b * LANES, LANES), :]
+
+        return Spread(n_tp, sp, tp, block, several, p_send.at[b], lambda group: p_recv.at[b, group])
 
     def pool(b, prior):
         low = b * LANES
@@ -320,6 +286,32 @@
 
     for b in range(1, blocks):
         pooled_spread(b).start()
+    for copy in inputs[:2] + inputs[6:]:
+        copy.wait()
+    for copy in loads:
+        copy.start()
+
+    high = max(16, experts)
+    route = [routes[k : k + 1, :] for k in range(TOPK)]
+    expert = lax.broadcasted_iota(jnp.int32, (high, length), 0)
+    used = sum((expert == route[k]).astype(jnp.float32) for k in range(TOPK))
+    before = lax.broadcasted_iota(jnp.int32, (length, length), 0) < lax.broadcasted_iota(
+        jnp.int32, (length, length), 1
+    )
+    taken = jnp.dot(
+        used.astype(jnp.bfloat16), before.astype(jnp.bfloat16), preferred_element_type=jnp.float32
+    )
+    slot = []
+    for k in range(TOPK):
+        rank = jnp.sum(jnp.where(expert == route[k], taken, 0.0), axis=0, keepdims=True)
+        slot.append(route[k].astype(jnp.float32) * cap + rank)
+    line = lax.broadcasted_iota(jnp.int32, (LANES, length), 0)
+    table = jnp.zeros((LANES, length), jnp.float32)
+    for k in range(TOPK):
+        table = jnp.where(line == k, slot[k], table)
+    columns = table.T
+    slot_column = [columns[:, k : 1 + k] for k in range(TOPK)]
+
     @pl.when(sp == 0)
     def _():
         halo[...] = jnp.zeros_like(halo)
@@ -377,23 +369,45 @@
             value = value + jnp.where(i == at, b + (a - b) * inner, 0)
         return value
 
-    def dispatch(chip, core):
+    held = chips == 4
+
+    def group(k):
+        return 0 if k == 0 else 2 if held and k == 2 else 1
+
+    def dispatch(k, core):
         return remote(
-            send.at[chip, core],
+            send.at[source(k), core],
             rows.at[my_chip, tp, my_core],
-            d_send.at[chip * CORES + core],
-            d_recv.at[sp],
-            (chip * CORES + core, tp),
+            d_send.at[group(k)],
+            d_recv.at[my_chip],
+            (source(k) * CORES + core, tp),
         )
 
-    def dispatch_scale(chip, core):
+    def dispatch_scale(k, core):
         return remote(
-            scale_send.at[chip, core],
+            scale_send.at[source(k), core],
             scale_rows.at[my_chip, my_core],
-            e_send.at[chip * CORES + core],
-            e_recv.at[sp],
-            (chip * CORES + core, tp),
+            e_send.at[group(k)],
+            e_recv.at[my_chip],
+            (source(k) * CORES + core, tp),
         )
+
+    partner = (my_chip * CORES + 1 - my_core, tp)
+
+    def dispatched(at):
+        few = [1, 2] if held else [1, chips - 1]
+        for buf, sem in ((send, d_send), (scale_send, e_send)):
+            ref = buf.at[0, 0] if at == 0 else buf.at[0] if at == 2 else buf.at[pl.ds(0, few[1])]
+            remote(ref, ref, sem.at[at], d_recv.at[0], partner).wait_send()
+
+    def arrived(chip, sem, both, one):
+        @pl.when(chip != my_chip)
+        def _():
+            remote(both, both, sem.at[chip], sem.at[chip], partner).wait_recv()
+
+        @pl.when(chip == my_chip)
+        def _():
+            remote(one, one, sem.at[chip], sem.at[chip], partner).wait_recv()
 
     place = lax.broadcasted_iota(jnp.int32, (flat, length), 0).astype(jnp.float32)
 
@@ -405,19 +419,20 @@
         send[chip] = chosen.reshape(CORES, cap, cols)
         if k == 0:
             rows[my_chip, tp, my_core] = send[my_chip, my_core]
-            dispatch(my_chip, 1 - my_core).start()
+            dispatch(0, 1 - my_core).start()
 
     def start_send(k, cores):
         for core in cores:
-            dispatch(source(k), core).start()
+            dispatch(k, core).start()
 
     def spread_of(buf, ssem, rsem, chip):
         def block(owner, piece):
             return buf.at[chip, owner, piece] if relay else buf.at[chip, owner]
 
-        return Spread(
-            n_tp, sp, tp, block, lambda i: ssem.at[chip, i], lambda owner, piece: rsem.at[chip, owner, piece]
-        )
+        def several(count):
+            return buf.at[chip, pl.ds(0, count)]
+
+        return Spread(n_tp, sp, tp, block, several, ssem.at[chip], lambda group: rsem.at[chip, group])
 
     def row_spread(chip):
         return spread_of(rows, f_send, f_recv, chip)
@@ -425,23 +440,14 @@
     def act_spread(chip):
         return spread_of(act, a_send, a_recv, chip)
 
+    def await_rows(chip):
+        arrived(chip, d_recv, rows.at[chip, tp], rows.at[chip, tp, 0])
+
     def start_rows(chip):
-        for core in range(CORES):
-
-            @pl.when(chip * CORES + core != sp)
-            def _():
-                remote(
-                    send.at[chip, core],
-                    rows.at[chip, tp, core],
-                    d_send.at[0],
-                    d_recv.at[chip * CORES + core],
-                    (chip * CORES + core, tp),
-                ).wait_recv()
-
+        await_rows(chip)
         row_spread(chip).start()
 
     first, rest = send_order(chips)
-    held = chips == 4
 
     def send_first(k):
         choose(k)
@@ -454,23 +460,46 @@
         def _():
             send_first(3)
 
-    for k in first:
-        send_first(k)
+    def start_own(core):
+        @pl.when(my_core == core)
+        def _():
+            if core == 1 and relay:
+                await_rows(my_chip)
+                for copy in row_spread(my_chip).direct()[0::3]:
+                    copy.start()
+            else:
+                start_rows(my_chip)
+
+    send_first(0)
     squares = jnp.sum(acc[...] * acc[...], axis=1, keepdims=True)
     own = jnp.broadcast_to(squares, (length, LANES)).T[0:8]
     mine[...] = own
     small = [
-        remote(mine, sums.at[tp], s_send.at[j - 1], s_recv.at[tp], (sp, lax.rem(tp + j, n_tp)))
+        remote(mine, sums.at[tp], s_send.at[0], s_recv.at[0], (sp, lax.rem(tp + j, n_tp)))
         for j in range(1, n_tp)
     ]
     for copy in small:
         copy.start()
-    start_rows(my_chip)
-
+
+    def all_sums():
+        ref = sums.at[pl.ds(0, n_tp - 1)]
+        return remote(ref, ref, s_send.at[0], s_recv.at[0], (sp, lax.rem(tp + 1, n_tp)))
+
+    start_own(0)
+    if relay:
+
+        @pl.when(my_core == 1)
+        def _():
+            for copy in row_spread(my_chip).direct()[1:3]:
+                copy.start()
+
+    for k in first[1:]:
+        send_first(k)
+    start_own(1)
+
+    all_sums().wait_recv()
     for j in range(1, n_tp):
-        owner = lax.rem(tp + n_tp - j, n_tp)
-        remote(mine, sums.at[owner], s_send.at[0], s_recv.at[owner], (sp, owner)).wait_recv()
-        own = own + sums[owner]
+        own = own + sums[lax.rem(tp + n_tp - j, n_tp)]
     scale = lax.rsqrt(own[0:1] / (cols * n_tp) + EPS)
     slots_here = lax.broadcasted_iota(jnp.int32, (room, length), 0).astype(jnp.float32)
     for k in first + rest:
@@ -478,9 +507,15 @@
         for core in range(CORES):
             here = slots_here + (chip * flat + core * cap).astype(jnp.float32)
             mine_here = sum(jnp.where(here == slot[j], scale, 0.0) for j in range(TOPK))
-            column = jnp.sum(mine_here, axis=1, keepdims=True)
-            line = jnp.broadcast_to(column, (room, LANES)).T[0:8]
-            scale_send[chip, core] = line
+            weigh = sum(
+                jnp.where(here == slot[j], route_weights[j : j + 1, :], 0.0) for j in range(TOPK)
+            )
+            pair = jnp.where(
+                lax.broadcasted_iota(jnp.int32, (room, LANES), 1) == 0,
+                jnp.sum(mine_here, axis=1, keepdims=True),
+                jnp.sum(weigh, axis=1, keepdims=True),
+            )
+            scale_send[chip, core] = pair.T[0:8]
 
             @pl.when(chip * CORES + core == sp)
             def _():
@@ -488,7 +523,7 @@
 
             @pl.when(chip * CORES + core != sp)
             def _():
-                dispatch_scale(chip, core).start()
+                dispatch_scale(k, core).start()
 
     for k in rest:
 
@@ -499,10 +534,7 @@
     def hold(chip):
         @pl.when(inner == 1)
         def _():
-            for k in (1, 3):
-                for core in range(CORES):
-                    dispatch(source(k), core).wait_send()
-                    dispatch_scale(source(k), core).wait_send()
+            dispatched(1)
             for k in (1, 2, 3):
                 for core in range(CORES):
                     pl.semaphore_signal(
@@ -521,34 +553,26 @@
         return remote(
             prod.at[chip, core, :, at],
             ret.at[my_chip, my_core, :, at],
-            r_send.at[chip * CORES + core],
-            r_recv.at[sp],
+            r_send.at[chip],
+            r_recv.at[my_chip],
             (chip * CORES + core, tp),
         )
 
     tile = min(hidden, 256)
     wide = min(cols, 256)
 
-    def activate(chip):
-        for core in range(CORES):
-
-            @pl.when(chip * CORES + core != sp)
-            def _():
-                remote(
-                    scale_send.at[chip, core],
-                    scale_rows.at[chip, core],
-                    e_send.at[0],
-                    e_recv.at[chip * CORES + core],
-                    (chip * CORES + core, tp),
-                ).wait_recv()
-
-        column = jnp.concatenate(
+    def slot_numbers(chip, which):
+        return jnp.concatenate(
             [
-                jnp.broadcast_to(scale_rows[chip, core, 0:1], (LANES, room)).T[:cap, 0:1]
+                jnp.broadcast_to(scale_rows[chip, core, which : which + 1], (LANES, room)).T[:cap, 0:1]
                 for core in range(CORES)
             ],
             axis=0,
         )
+
+    def activate(chip):
+        arrived(chip, e_recv, scale_rows.at[chip], scale_rows.at[chip, 0])
+        column = slot_numbers(chip, 0)
 
         @pl.loop(0, hidden // tile)
         def _(n):
@@ -563,15 +587,34 @@
             value = (jax.nn.silu(gate * column) * (up * column)).astype(jnp.bfloat16)
             act[chip, tp, :, :, at] = value.reshape(CORES, cap, tile)
 
-    def produce(chip):
+    def products(chip, owners, at):
+        total = jnp.zeros((flat, wide), jnp.float32)
+        for t in owners:
+            block = act[chip, t].reshape(flat, hidden)
+            deep = pl.ds(pl.multiple_of(t * hidden, hidden), hidden)
+            total += jnp.dot(block, w_down[deep, at], preferred_element_type=jnp.float32)
+        return total
+
+    if relay:
+        near, far = [tp, 2 * (tp // 2) + 1 - tp % 2, (tp + 2) % 4], [3 - tp]
+    else:
+        near, far = [tp], [lax.rem(tp + j, n_tp) for j in range(1, n_tp)]
+
+    def tiles(n):
+        return pl.ds(pl.multiple_of(n * wide, wide), wide)
+
+    def produce_near(chip):
         @pl.loop(0, cols // wide)
         def _(n):
-            at = pl.ds(pl.multiple_of(n * wide, wide), wide)
-            total = jnp.zeros((flat, wide), jnp.float32)
-            for t in range(n_tp):
-                block = act[chip, t].reshape(flat, hidden)
-                deep = pl.ds(t * hidden, hidden)
-                total += jnp.dot(block, w_down[deep, at], preferred_element_type=jnp.float32)
+            partial[:, tiles(n)] = products(chip, near, tiles(n))
+
+    def produce(chip):
+        weigh = slot_numbers(chip, 1)
+
+        @pl.loop(0, cols // wide)
+        def _(n):
+            at = tiles(n)
+            total = (partial[:, at] + products(chip, far, at)) * weigh
             prod[chip, :, :, at] = total.astype(jnp.bfloat16).reshape(CORES, cap, wide)
             for core in range(CORES):
 
@@ -586,6 +629,7 @@
 
     def finish_act(chip):
         act_spread(chip).finish_near()
+        produce_near(chip)
         act_spread(chip).finish()
         produce(chip)
 
@@ -595,29 +639,41 @@
 
     lane = lax.broadcasted_iota(jnp.int32, (length, flat), 1).astype(jnp.float32)
 
+    def returned(chip):
+        here = lane + (chip * flat).astype(jnp.float32)
+        pick = sum((slot_column[j] == here).astype(jnp.float32) for j in range(TOPK)).astype(jnp.bfloat16)
+        arrived(chip, r_recv, ret.at[chip], ret.at[chip, 0])
+        return acc[...] + jnp.dot(pick, ret[chip].reshape(flat, cols), preferred_element_type=jnp.float32)
+
     def combine(chip):
-        here = lane + (chip * flat).astype(jnp.float32)
-        weight = sum(
-            jnp.where(slot_column[j] == here, weight_column[j], 0.0) for j in range(TOPK)
-        )
-        upper = weight.astype(jnp.bfloat16)
-        lower = (weight - upper.astype(jnp.float32)).astype(jnp.bfloat16)
-        for core in range(CORES):
-
-            @pl.when(chip * CORES + core != sp)
+        acc[...] = returned(chip)
+
+    def combine_last(chip):
+        out[...] = returned(chip)
+
+    def settle(_chip):
+        @pl.when(sp < n_sp - 1)
+        def _():
+            for copy in halo_copies(sp + 1):
+                copy.wait_send()
+
+        all_sums().wait_send()
+        for b in range(blocks):
+            pooled_spread(b).sent()
+        dispatched(0)
+        if held:
+
+            @pl.when(inner == 0)
             def _():
-                remote(
-                    prod.at[chip, core],
-                    ret.at[chip, core],
-                    r_send.at[0],
-                    r_recv.at[chip * CORES + core],
-                    (chip * CORES + core, tp),
-                ).wait_recv()
-
-        back = ret[chip].reshape(flat, cols)
-        acc[...] += jnp.dot(upper, back, preferred_element_type=jnp.float32) + jnp.dot(
-            lower, back, preferred_element_type=jnp.float32
-        )
+                dispatched(1)
+
+            dispatched(2)
+        else:
+            dispatched(1)
+
+        @pl.loop(0, chips)
+        def _(chip):
+            row_spread(chip).sent()
 
     stages = [
         start_rows,
@@ -628,6 +684,8 @@
         finish_act,
         combine,
         hold,
+        combine_last,
+        settle,
     ]
     mid, edge = [
         [STAGES.index(name) * chips + k for name, k in steps] for steps in schedules(chips)
@@ -645,34 +703,17 @@
             def _():
                 stage(chip)
 
-    out[...] = acc[...]
-
-    @pl.when(sp < n_sp - 1)
-    def _():
-        for copy in halo_copies(sp + 1):
-            copy.wait_send()
-
-    for copy in small:
-        copy.wait_send()
-    for b in range(blocks):
-        pooled_spread(b).sent()
-    for copy in (dispatch, dispatch_scale, give_back):
-        copy(my_chip, 1 - my_core).wait_send()
-
-    @pl.loop(1, chips)
-    def _(k):
-        for core in range(CORES):
-            give_back(source(k), core).wait_send()
-
-            @pl.when((inner == 0) | (k == 2) | (not held))
-            def _():
-                for copy in (dispatch, dispatch_scale):
-                    copy(source(k), core).wait_send()
-
     @pl.loop(0, chips)
     def _(chip):
-        row_spread(chip).sent()
         act_spread(chip).sent()
+
+        @pl.when(chip != my_chip)
+        def _():
+            remote(prod.at[chip], prod.at[chip], r_send.at[chip], r_recv.at[0], partner).wait_send()
+
+        @pl.when(chip == my_chip)
+        def _():
+            remote(prod.at[chip, 0], prod.at[chip, 0], r_send.at[chip], r_recv.at[0], partner).wait_send()
 
 
 def shards(
@@ -697,8 +738,7 @@
     cap = length * TOPK * 3 // (2 * n_sp)
     room = -(-cap // LANES) * LANES
     blocks = length // LANES
-    pieces = 2 if n_tp == 4 else 1
-    fan = 6 if n_tp == 4 else n_tp
+    groups = 3 if n_tp == 4 else 1
     dma = pltpu.SemaphoreType.DMA
     vmem = pl.BlockSpec(memory_space=pltpu.VMEM)
     hbm = pl.BlockSpec(memory_space=pl.ANY)
@@ -731,6 +771,7 @@
             pltpu.VMEM((chips, CORES, cap, cols), half),
             pltpu.VMEM((chips, CORES, 8, room), jnp.float32),
             pltpu.VMEM((chips, CORES, 8, room), jnp.float32),
+            pltpu.VMEM((CORES * cap, cols), jnp.float32),
             pltpu.VMEM(out_weight.shape, half),
             pltpu.VMEM(w_gate.shape[1:], half),
             pltpu.VMEM(w_up.shape[1:], half),
@@ -739,20 +780,20 @@
             dma((4,)),
             dma((2,)),
             dma((2,)),
-            dma((blocks, fan)),
-            dma((blocks, n_tp, pieces)),
-            dma((n_tp,)),
-            dma((n_tp,)),
-            dma((n_sp,)),
-            dma((n_sp,)),
-            dma((chips, fan)),
-            dma((chips, n_tp, pieces)),
-            dma((chips, fan)),
-            dma((chips, n_tp, pieces)),
-            dma((n_sp,)),
-            dma((n_sp,)),
-            dma((n_sp,)),
-            dma((n_sp,)),
+            dma((blocks,)),
+            dma((blocks, groups)),
+            dma((1,)),
+            dma((1,)),
+            dma((3,)),
+            dma((chips,)),
+            dma((chips,)),
+            dma((chips, groups)),
+            dma((chips,)),
+            dma((chips, groups)),
+            dma((chips,)),
+            dma((chips,)),
+            dma((3,)),
+            dma((chips,)),
             pltpu.SemaphoreType.REGULAR,
         ],
         compiler_params=pltpu.CompilerParams(

time: 106 us -> 102 us (0.962)
  Pallas kernels: 104 us -> 101 us
    pallas_call x1, Pallas kernels: 104 us -> 101 us  [shards(): pl.pallas_call(functools.partial(layer_kernel, n_sp, n_tp), out_shape=plt...]
where the time goes in v4:
time: 102 us
  Pallas kernels  101 us (99%)
    pallas_call x1, Pallas kernels, shards(): pl.pallas_call(functools.partial(layer_kernel, n_sp, n_tp), out_shape=plt...  101 us

profile of v4, /device:TPU:1, one launch (start us, length us, event | category | flops | bytes accessed | tf_op | source)
XLA Modules:
  0.0 101.9 jit_solution(468408089930607637)
XLA Ops:
  0.0 101.0 %shard_map.118 = f32[256,1024]{1,0:T(8,128)S(1)} custom-call(bf16[256,1024]{1,0:T(8,128)(2,1)} %residual_hbm.1, bf16[256,512]{1,0:T(8,128)(2,1)} %pool_in_hbm.1, s32[1,256]{1,0:T(1,128)} %bitcast.15, bf16[4,128,128]{2,1,0:T(8,128)(2,1)} %pool_weight_hbm.1, f32[1,512]{1,0:T(1,128)} %bitcast.12, f32[1,4096]{1,0:T(1,128)} %bitcast.11, s32[2,256]{1,0:T(2,128)} %bitcast.13, ...), custom_call_target="tpu_custom_call" | custom-call | tf_op jit(solution)/shard_map/pallas_call | solution.py:746
  101.0 0.9 convert_element_type.3

commit v5 on v4

--- a/solution.py
+++ b/solution.py
@@ -84,9 +84,9 @@
     "RD0 Z0 D3 RD3",
     "D1 CD3 A3 RA3",
     "D2 CD0 CA3 RD2",
-    "RD1 CD2 A2 CD1",
-    "RA2 A1 CA2 RA1",
-    "A0 C3 CA1 RA0",
+    "RD1 CD2 A2 RA2",
+    "CD1 A1 CA2 RA1",
+    "A0 CA1 C3 RA0",
     "C1 W0 CA0 C0",
     "E2",
 )
@@ -226,7 +226,7 @@
 
     doc_row = docs[...].astype(jnp.float32)
     doc_column = jnp.broadcast_to(doc_row, (LANES, length)).T[:, 0:1]
-    ext[0 : LANES - TAIL, :] = jnp.zeros((LANES - TAIL, width), jnp.bfloat16)
+    ext[0:LANES, :] = jnp.zeros((LANES, width), jnp.bfloat16)
     ext[LANES:, :] = pool_in[...]
 
     blocks = length // LANES
@@ -248,7 +248,7 @@
 
         return Spread(n_tp, sp, tp, block, several, p_send.at[b], lambda group: p_recv.at[b, group])
 
-    def pool(b, prior):
+    def pool(b, prior, begin=0, end=LANES):
         low = b * LANES
         near = (doc_column[low : low + LANES, :] == prior) & (away >= 0)
         groups = width // GD
@@ -266,7 +266,8 @@
             own = ext[low + LANES : low + 2 * LANES, at].astype(jnp.float32)
             diff = (total / count - own).astype(jnp.bfloat16)
             mixed = jnp.dot(diff, pool_weight[g], preferred_element_type=jnp.float32)
-            gathered[tp, low : low + LANES, at] = (mixed * pool_gain[:, at]).astype(jnp.bfloat16)
+            pooled = (mixed * pool_gain[:, at]).astype(jnp.bfloat16)
+            gathered[tp, low + begin : low + end, at] = pooled[begin:end]
 
     for b in range(1, blocks):
         pool(b, doc_row[:, (b - 1) * LANES : (b + 1) * LANES])
@@ -312,6 +313,12 @@
     columns = table.T
     slot_column = [columns[:, k : 1 + k] for k in range(TOPK)]
 
+    none = jnp.full((1, LANES), -1.0, jnp.float32)
+    if relay:
+        pool(0, jnp.concatenate([none, doc_row[:, :LANES]], axis=1), half, LANES)
+        for copy in pooled_spread(0).direct()[1:3]:
+            copy.start()
+
     @pl.when(sp == 0)
     def _():
         halo[...] = jnp.zeros_like(halo)
@@ -324,8 +331,9 @@
 
     ext[LANES - TAIL : LANES, :] = halo[...]
     first_docs = halo_docs[...].astype(jnp.float32)
-    pool(0, jnp.concatenate([first_docs, doc_row[:, :LANES]], axis=1))
-    pooled_spread(0).start()
+    pool(0, jnp.concatenate([first_docs, doc_row[:, :LANES]], axis=1), 0, half if relay else LANES)
+    for copy in pooled_spread(0).direct()[0 :: 3 if relay else 1]:
+        copy.start()
 
     def part(owner):
         deep = pl.ds(pl.multiple_of(owner * width, width), width)
@@ -649,7 +657,7 @@
         acc[...] = returned(chip)
 
     def combine_last(chip):
-        out[...] = returned(chip)
+        out[...] = returned(chip).astype(jnp.bfloat16)
 
     def settle(_chip):
         @pl.when(sp < n_sp - 1)
@@ -745,7 +753,7 @@
     half = jnp.bfloat16
     return pl.pallas_call(
         functools.partial(layer_kernel, n_sp, n_tp),
-        out_shape=pltpu.VMEM((length, cols), jnp.float32),
+        out_shape=pltpu.VMEM((length, cols), half),
         in_specs=[hbm] * 12,
         out_specs=vmem,
         scratch_shapes=[
@@ -812,7 +820,7 @@
         w_gate[0],
         w_up[0],
         w_down[0],
-    ).astype(half)
+    )
 
 
 def solution(mesh):

time: 102 us -> 102 us (level)
  no operation moved by 1% of the time
where the time goes in v5:
time: 102 us
  Pallas kernels  101 us (99%)
    pallas_call x1, Pallas kernels, shards(): pl.pallas_call(functools.partial(layer_kernel, n_sp, n_tp), out_shape=plt...  101 us

profile of v5, /device:TPU:1, one launch (start us, length us, event | category | flops | bytes accessed | tf_op | source)
XLA Modules:
  0.0 101.6 jit_solution(6418194233397380893)
XLA Ops:
  0.0 100.8 %shard_map.118 = bf16[256,1024]{1,0:T(8,128)(2,1)S(1)} custom-call(bf16[256,1024]{1,0:T(8,128)(2,1)} %residual_hbm.1, bf16[256,512]{1,0:T(8,128)(2,1)} %pool_in_hbm.1, s32[1,256]{1,0:T(1,128)} %bitcast.15, bf16[4,128,128]{2,1,0:T(8,128)(2,1)} %pool_weight_hbm.1, f32[1,512]{1,0:T(1,128)} %bitcast.12, f32[1,4096]{1,0:T(1,128)} %bitcast.11, s32[2,256]{1,0:T(2,128)} %bitcast.13, ...), custom_call_target="tpu_custom_call" | custom-call | tf_op jit(solution)/shard_map/pallas_call | solution.py:754
  100.8 0.8 copy.14

commit v6 on v5

--- a/solution.py
+++ b/solution.py
@@ -29,7 +29,8 @@
 
 
 class Spread:
-    def __init__(self, n_tp, sp, tp, block, blocks, send_sem, recv_sem):
+    def __init__(self, n_tp, sp, tp, block, blocks, send_sem, recv_sem, apart=0):
+        self.apart = apart
         self.n_tp, self.sp, self.tp = n_tp, sp, tp
         self.block, self.blocks, self.send_sem, self.recv_sem = block, blocks, send_sem, recv_sem
         self.relay = n_tp == 4
@@ -45,7 +46,7 @@
         if self.relay:
             return [
                 self.copy(self.tp, 0, 0, self.across),
-                self.copy(self.tp, 1, 0, self.along),
+                self.copy(self.tp, 1, self.apart, self.along),
                 self.copy(self.tp, 1, 1, self.across),
                 self.copy(self.tp, 0, 1, self.along),
             ]
@@ -64,6 +65,11 @@
             self.all_of(0, 1).wait_recv()
             self.copy(self.across, 0, 2, self.along).start()
             self.copy(self.along, 1, 2, self.across).start()
+
+    def pass_piece(self, piece):
+        owner, peer = (self.across, self.along) if piece == 0 else (self.along, self.across)
+        self.copy(owner, piece, self.apart * piece, peer).wait_recv()
+        self.copy(owner, piece, 2, peer).start()
 
     def finish_near(self):
         if self.relay:
@@ -235,42 +241,46 @@
         + lax.broadcasted_iota(jnp.int32, (LANES, 2 * LANES), 0)
         - lax.broadcasted_iota(jnp.int32, (LANES, 2 * LANES), 1)
     )
-    half = LANES // 2
 
     def pooled_spread(b):
         def block(owner, piece):
+            if relay and piece == min(b, 1):
+                return gathered.at[owner, pl.ds(b * LANES, TAIL), :]
             if relay:
-                return gathered.at[owner, pl.ds(b * LANES + piece * half, half), :]
+                return gathered.at[owner, pl.ds(b * LANES + TAIL, LANES - TAIL), :]
             return gathered.at[owner, pl.ds(b * LANES, LANES), :]
 
         def several(count):
             return gathered.at[pl.ds(0, count), pl.ds(b * LANES, LANES), :]
 
-        return Spread(n_tp, sp, tp, block, several, p_send.at[b], lambda group: p_recv.at[b, group])
+        return Spread(n_tp, sp, tp, block, several, p_send.at[b], lambda group: p_recv.at[b, group], 3)
 
     def pool(b, prior, begin=0, end=LANES):
         low = b * LANES
-        near = (doc_column[low : low + LANES, :] == prior) & (away >= 0)
+        near = (doc_column[low + begin : low + end, :] == prior) & (away[begin:end] >= 0)
         groups = width // GD
         for g in range(groups):
             if groups % 4 == 0:
                 span = 2 << (g % 4)
             else:
                 span = lax.shift_left(jnp.int32(2), (tp * groups + g) % 4)
-            weight = (near & (away < span)).astype(jnp.float32)
+            weight = (near & (away[begin:end] < span)).astype(jnp.float32)
             at = slice(g * GD, (g + 1) * GD)
             count = jnp.sum(weight, axis=1, keepdims=True)
             total = jnp.dot(
                 weight.astype(jnp.bfloat16), ext[low : low + 2 * LANES, at], preferred_element_type=jnp.float32
             )
-            own = ext[low + LANES : low + 2 * LANES, at].astype(jnp.float32)
+            own = ext[low + LANES + begin : low + LANES + end, at].astype(jnp.float32)
             diff = (total / count - own).astype(jnp.bfloat16)
             mixed = jnp.dot(diff, pool_weight[g], preferred_element_type=jnp.float32)
             pooled = (mixed * pool_gain[:, at]).astype(jnp.bfloat16)
-            gathered[tp, low + begin : low + end, at] = pooled[begin:end]
+            gathered[tp, low + begin : low + end, at] = pooled
 
     for b in range(1, blocks):
         pool(b, doc_row[:, (b - 1) * LANES : (b + 1) * LANES])
+    if relay:
+        none = jnp.full((1, LANES), -1.0, jnp.float32)
+        pool(0, jnp.concatenate([none, doc_row[:, :LANES]], axis=1), TAIL, LANES)
 
     pl.semaphore_wait(barrier, len(peers))
 
@@ -285,8 +295,19 @@
         for copy in halo_copies(sp + 1):
             copy.start()
 
-    for b in range(1, blocks):
-        pooled_spread(b).start()
+    later = range(1, blocks)
+    if relay:
+        for b in later:
+            pooled_spread(b).direct()[1].start()
+            pooled_spread(b).direct()[0].start()
+        for copy in pooled_spread(0).direct()[1:3]:
+            copy.start()
+        for b in later:
+            for copy in pooled_spread(b).direct()[2:4]:
+                copy.start()
+    else:
+        for b in later:
+            pooled_spread(b).start()
     for copy in inputs[:2] + inputs[6:]:
         copy.wait()
     for copy in loads:
@@ -313,12 +334,6 @@
     columns = table.T
     slot_column = [columns[:, k : 1 + k] for k in range(TOPK)]
 
-    none = jnp.full((1, LANES), -1.0, jnp.float32)
-    if relay:
-        pool(0, jnp.concatenate([none, doc_row[:, :LANES]], axis=1), half, LANES)
-        for copy in pooled_spread(0).direct()[1:3]:
-            copy.start()
-
     @pl.when(sp == 0)
     def _():
         halo[...] = jnp.zeros_like(halo)
@@ -331,7 +346,7 @@
 
     ext[LANES - TAIL : LANES, :] = halo[...]
     first_docs = halo_docs[...].astype(jnp.float32)
-    pool(0, jnp.concatenate([first_docs, doc_row[:, :LANES]], axis=1), 0, half if relay else LANES)
+    pool(0, jnp.concatenate([first_docs, doc_row[:, :LANES]], axis=1), 0, TAIL if relay else LANES)
     for copy in pooled_spread(0).direct()[0 :: 3 if relay else 1]:
         copy.start()
 
@@ -342,9 +357,13 @@
     loads[0].wait()
     acc[...] = residual[...].astype(jnp.float32) + part(tp)
     late_first = list(range(1, blocks)) + [0]
-    for b in late_first:
-        pooled_spread(b).pass_on()
     if relay:
+        for b in later:
+            pooled_spread(b).pass_piece(0)
+        pooled_spread(0).pass_piece(1)
+        for b in later:
+            pooled_spread(b).pass_piece(1)
+        pooled_spread(0).pass_piece(0)
         for b in late_first:
             pooled_spread(b).finish_near()
         acc[...] += part(2 * (tp // 2) + 1 - tp % 2)
@@ -789,7 +808,7 @@
             dma((2,)),
             dma((2,)),
             dma((blocks,)),
-            dma((blocks, groups)),
+            dma((blocks, groups + 1)),
             dma((1,)),
             dma((1,)),
             dma((3,)),

time: 102 us -> 102 us (level)
  no operation moved by 1% of the time
where the time goes in v6:
time: 102 us
  Pallas kernels  101 us (99%)
    pallas_call x1, Pallas kernels, shards(): pl.pallas_call(functools.partial(layer_kernel, n_sp, n_tp), out_shape=plt...  101 us

profile of v6, /device:TPU:1, one launch (start us, length us, event | category | flops | bytes accessed | tf_op | source)
XLA Modules:
  0.0 101.6 jit_solution(5915725596972251859)
XLA Ops:
  0.0 100.8 %shard_map.118 = bf16[256,1024]{1,0:T(8,128)(2,1)S(1)} custom-call(bf16[256,1024]{1,0:T(8,128)(2,1)} %residual_hbm.1, bf16[256,512]{1,0:T(8,128)(2,1)} %pool_in_hbm.1, s32[1,256]{1,0:T(1,128)} %bitcast.15, bf16[4,128,128]{2,1,0:T(8,128)(2,1)} %pool_weight_hbm.1, f32[1,512]{1,0:T(1,128)} %bitcast.12, f32[1,4096]{1,0:T(1,128)} %bitcast.11, s32[2,256]{1,0:T(2,128)} %bitcast.13, ...), custom_call_target="tpu_custom_call" | custom-call | tf_op jit(solution)/shard_map/pallas_call | solution.py:773
  100.8 0.8 copy.14
